TPU v7x, 256 devices: a whole 4x4x8 slice. The times are simulated.
256 devices in a mesh: ep: 64 (over z, y, x_hi), tp: 4 (over x_lo, core).
Axes of the slice: x: 4 (x_hi: 2, x_lo: 2; x = x_hi * 2 + x_lo), y: 4, z: 8, core: 2. Of those that a mesh axis runs over, the one named last changes fastest.
Arguments:
- tokens: bfloat16 [1536, 2048], P('ep'), may hold values from -6 to 6
- delta_state: float32 [1536, 8, 128, 128], P('ep', 'tp'), may hold values from -3 to 3
- first_gain: bfloat16 [2048], replicated, may hold values from 0.099609375 to 1.8984375
- query_weight: bfloat16 [2048, 1024], P(None, 'tp'), may hold values from -0.125 to 0.125
- key_weight: bfloat16 [2048, 1024], P(None, 'tp'), may hold values from -0.125 to 0.125
- value_weight: bfloat16 [2048, 1024], P(None, 'tp'), may hold values from -0.125 to 0.125
- outgate_weight: bfloat16 [2048, 1024], P(None, 'tp'), may hold values from -0.125 to 0.125
- beta_weight: bfloat16 [2048, 8], replicated, may hold values from -0.125 to 0.125
- decay_weight: bfloat16 [2048, 8], replicated, may hold values from -0.125 to 0.125
- decay_rate: float32 [8], replicated, may hold values from 0.05 to 4
- decay_bias: float32 [8], replicated, may hold values from -3 to 3
- head_gain: bfloat16 [128], replicated, may hold values from 0.099609375 to 1.8984375
- out_weight: bfloat16 [1024, 2048], P('tp'), may hold values from -0.1875 to 0.1875
- second_gain: bfloat16 [2048], replicated, may hold values from 0.099609375 to 1.8984375
- blend_weight: bfloat16 [2048], replicated, may hold values from -0.125 to 0.125
- dense_gate_weight: bfloat16 [2048, 2048], P(None, 'tp'), may hold values from -0.125 to 0.125
- dense_up_weight: bfloat16 [2048, 2048], P(None, 'tp'), may hold values from -0.125 to 0.125
- dense_down_weight: bfloat16 [2048, 2048], P('tp'), may hold values from -0.125 to 0.125
- expert_gate: bfloat16 [256, 2048, 512], P(('ep', 'tp')), may hold values from -0.125 to 0.125
- expert_up: bfloat16 [256, 2048, 512], P(('ep', 'tp')), may hold values from -0.125 to 0.125
- expert_down: bfloat16 [256, 512, 2048], P(('ep', 'tp')), may hold values from -0.25 to 0.25
- route_ids: int32 [1536, 6], P('ep'), may hold values from 0 to 255, all different within a row; in each aligned block of 24 rows (0 to 23, 24 to 47, ...) at most 2 rows name the same one
- route_weights: float32 [1536, 6], P('ep'), may hold values from 0.1 to 1
Outputs:
- new_tokens: bfloat16 [1536, 2048], P('ep')
- new_state: float32 [1536, 8, 128, 128], P('ep', 'tp')
Inputs may be any that keep to these rules, and one draw needn't show every extreme that they name: `route_ids`: each row names 6 different experts. In each aligned block of 24 rows (the sequences of one index of ep) no expert is named by more than 2 rows, and in some block an expert is named by exactly 2 rows.
All inputs are finite; a program needn't handle non-finite values.
Results may differ from a plain program's by a relative error of at most 0.017.
Values may be sent and summed in bfloat16 or wider, within the bound.
A program may use at most 128 MiB of HBM per device.

v0:
```python
import jax
import jax.numpy as jnp
from jax import lax
from jax.sharding import PartitionSpec as P

norm_eps = 1e-06
unit_eps = 1e-06
routed_scale = 2.5


def over_pieces(x, axis):
    pieces = lax.all_gather(x, axis).astype(jnp.float32)
    return pieces.sum(axis=0)


def sent_to_all(x, axis):
    devices = lax.axis_size(axis)
    return lax.all_to_all(jnp.broadcast_to(x[None], (devices, *x.shape)), axis, 0, 0, tiled=True)


def over_copies(x, axis):
    return sent_to_all(x, axis).astype(jnp.float32).sum(axis=0)


def rms_scale(values, gain):
    values = values.astype(jnp.float32)
    inverse = lax.rsqrt(jnp.mean(values * values, axis=-1, keepdims=True) + norm_eps)
    return values * inverse * gain.astype(jnp.float32)


def unit_rows(values):
    return values * lax.rsqrt(jnp.sum(values * values, axis=-1, keepdims=True) + unit_eps)


def rounded(values):
    return lax.optimization_barrier(values.astype(jnp.bfloat16)).astype(jnp.float32)


def delta_update(delta_state, query_raw, key_raw, value_raw, beta_gate, log_decay):
    head_size = delta_state.shape[-1]
    query_unit = unit_rows(jax.nn.silu(query_raw)) * head_size ** (-0.5)
    key_unit = unit_rows(jax.nn.silu(key_raw))
    value_act = jax.nn.silu(value_raw)
    decayed = jnp.exp(log_decay)[:, :, None, None] * delta_state
    predicted = jnp.einsum("shkv,shk->shv", decayed, key_unit)
    update = (beta_gate[:, :, None] * key_unit)[:, :, :, None] * (value_act - predicted)[
        :, :, None, :
    ]
    new_state = decayed + update
    readout = jnp.einsum("shkv,shk->shv", new_state, query_unit)
    return (new_state, readout)


def gated_heads(readout, outgate_raw, head_gain):
    scaled = rms_scale(readout, head_gain) * jax.nn.silu(outgate_raw)
    return scaled.reshape(scaled.shape[0], -1).astype(jnp.bfloat16)


def expert_rows(row_block, gate_mat, up_mat, down_mat):
    gate_part = jnp.dot(row_block, gate_mat, preferred_element_type=jnp.float32)
    up_part = jnp.dot(row_block, up_mat, preferred_element_type=jnp.float32)
    hidden = (jax.nn.silu(gate_part) * up_part).astype(jnp.bfloat16)
    return jnp.dot(hidden, down_mat, preferred_element_type=jnp.float32).astype(jnp.bfloat16)


def shards(
    tokens,
    delta_state,
    first_gain,
    query_weight,
    key_weight,
    value_weight,
    outgate_weight,
    beta_weight,
    decay_weight,
    decay_rate,
    decay_bias,
    head_gain,
    out_weight,
    second_gain,
    blend_weight,
    dense_gate_weight,
    dense_up_weight,
    dense_down_weight,
    expert_gate,
    expert_up,
    expert_down,
    route_ids,
    route_weights,
):
    seq_count = tokens.shape[0]
    head_local = delta_state.shape[1]
    head_size = delta_state.shape[2]
    top_count = route_ids.shape[1]
    ep_count = lax.axis_size("ep")
    tp_count = lax.axis_size("tp")
    tp_index = lax.axis_index("tp")
    normed = rms_scale(tokens, first_gain).astype(jnp.bfloat16)

    def project(weight):
        product = jnp.dot(normed, weight, preferred_element_type=jnp.float32)
        return rounded(product).reshape(seq_count, head_local, head_size)

    query_raw = project(query_weight)
    key_raw = project(key_weight)
    value_raw = project(value_weight)
    outgate_raw = project(outgate_weight)
    head_start = tp_index * head_local
    beta_all = jax.nn.sigmoid(jnp.dot(normed, beta_weight, preferred_element_type=jnp.float32))
    beta_gate = lax.dynamic_slice_in_dim(beta_all, head_start, head_local, 1)
    decay_input = jnp.dot(normed, decay_weight, preferred_element_type=jnp.float32) + decay_bias
    decay_all = -decay_rate * jax.nn.softplus(decay_input)
    log_decay = lax.dynamic_slice_in_dim(decay_all, head_start, head_local, 1)
    new_state, readout = delta_update(
        delta_state, query_raw, key_raw, value_raw, beta_gate, log_decay
    )
    gated = gated_heads(readout, outgate_raw, head_gain)
    mix_part = jnp.dot(gated, out_weight, preferred_element_type=jnp.float32)
    mixed = over_pieces(mix_part.astype(jnp.bfloat16), "tp").astype(jnp.float32)
    residual = (tokens.astype(jnp.float32) + mixed).astype(jnp.bfloat16)
    normed_mid = rms_scale(residual, second_gain).astype(jnp.bfloat16)
    blend_gate = jax.nn.sigmoid(
        jnp.dot(normed_mid, blend_weight, preferred_element_type=jnp.float32)
    )
    dense_gate_raw = jnp.dot(normed_mid, dense_gate_weight, preferred_element_type=jnp.float32)
    dense_up_raw = jnp.dot(normed_mid, dense_up_weight, preferred_element_type=jnp.float32)
    dense_hidden = (jax.nn.silu(dense_gate_raw) * dense_up_raw).astype(jnp.bfloat16)
    dense_part = jnp.dot(dense_hidden, dense_down_weight, preferred_element_type=jnp.float32)
    expert_count = ep_count * tp_count
    capacity = max(2, (3 * seq_count * top_count + 2 * expert_count - 1) // (2 * expert_count))
    flat_ids = route_ids.reshape(-1)
    assign_count = flat_ids.shape[0]
    earlier = jnp.arange(assign_count)[:, None] > jnp.arange(assign_count)[None, :]
    matches = (flat_ids[:, None] == flat_ids[None, :]) & earlier
    rank_of = jnp.sum(matches.astype(jnp.int32), axis=1)
    owned = flat_ids % tp_count == tp_index
    slot_of = jnp.where(owned, flat_ids // tp_count * capacity + rank_of, -1)
    slot_total = ep_count * capacity
    slot_grid = slot_of.reshape(seq_count, top_count)
    slot_range = jnp.arange(slot_total, dtype=jnp.int32)
    dispatch = jnp.any(slot_grid[None, :, :] == slot_range[:, None, None], axis=2).astype(
        jnp.bfloat16
    )
    model_width = normed_mid.shape[1]
    outgoing = jnp.dot(dispatch, normed_mid, preferred_element_type=jnp.float32).astype(
        jnp.bfloat16
    )
    outgoing = outgoing.reshape(ep_count, capacity, model_width)
    arrived = lax.all_to_all(outgoing, "ep", split_axis=0, concat_axis=0, tiled=True)
    result = expert_rows(
        arrived.reshape(-1, model_width), expert_gate[0], expert_up[0], expert_down[0]
    )
    returned = lax.all_to_all(
        result.reshape(arrived.shape), "ep", split_axis=0, concat_axis=0, tiled=True
    )
    returned_rows = returned.reshape(slot_total, model_width)
    picked = returned_rows[jnp.maximum(slot_of, 0)].astype(jnp.float32)
    picked = picked.reshape(seq_count, top_count, model_width)
    route_scale = route_weights / jnp.sum(route_weights, axis=1, keepdims=True) * routed_scale
    kept_scale = jnp.where(owned.reshape(seq_count, top_count), route_scale, 0.0)
    routed_part = jnp.sum(kept_scale[:, :, None] * picked, axis=1)
    combined = over_copies(
        (routed_part + blend_gate[:, None] * dense_part).astype(jnp.bfloat16), "tp"
    ).astype(jnp.float32)
    new_tokens = (residual.astype(jnp.float32) + combined).astype(jnp.bfloat16)
    return (new_tokens, new_state)


def solution(mesh):
    placed = (
        P("ep", None),
        P("ep", "tp", None, None),
        P(),
        P(None, "tp"),
        P(None, "tp"),
        P(None, "tp"),
        P(None, "tp"),
        P(),
        P(),
        P(),
        P(),
        P(),
        P("tp", None),
        P(),
        P(),
        P(None, "tp"),
        P(None, "tp"),
        P("tp", None),
        P(("ep", "tp"), None, None),
        P(("ep", "tp"), None, None),
        P(("ep", "tp"), None, None),
        P("ep", None),
        P("ep", None),
    )
    return jax.shard_map(
        shards,
        mesh=mesh,
        in_specs=placed,
        out_specs=(P("ep", None), P("ep", "tp", None, None)),
        check_vma=False,
    )
```

profile of v0, /device:TPU:1, one launch (start us, length us, event | category | flops | bytes accessed | tf_op | source)
XLA Modules:
  0.0 109.6 jit_solution(5367061146839519999)
XLA Ops:
  0.6 0.0 copy-start
  0.6 0.0 copy-start.3
  0.7 0.0 copy-start.4
  0.7 0.8 convert_element_type.87
  1.5 1.1 fusion.31
  2.6 0.7 neg.38
  3.3 1.1 %fusion.21 = f32[24,8]{0,1:T(8,128)S(1)} fusion(bf16[2048,8]{0,1:T(8,128)(2,1)} %param.30, bf16[24,2048]{1,0:T(8,128)(2,1)} %param.23, f32[2048]{0:T(1024)S(1)} %convert_element_type.87, f32[24]{0:T(128)S(1)} %add_rsqrt_fusion.4), kind=kOutput, calls=%fused_computation.28 | convolution fusion | flops 983616 | bytes 140128 | tf_op jit(solution)/shard_map/dot_general | solution.py:109
  4.4 1.2 %fusion.59 = f32[24,8]{0,1:T(8,128)S(1)} fusion(bf16[2048,8]{0,1:T(8,128)(2,1)} %param.31, f32[8]{0:T(128)} %param.33, f32[8]{0:T(128)S(1)} %neg.38, bf16[24,2048]{1,0:T(8,128)(2,1)} %param.23, f32[2048]{0:T(1024)S(1)} %convert_element_type.87, f32[24]{0:T(128)S(1)} %add_rsqrt_fusion.4), kind=kOutput, calls=%fused_computation.100 | convolution fusion | flops 984576 | bytes 140192 | tf_op jit(solution)/shard_map/dot_general | solution.py:111
  5.6 0.1 copy.39
  5.6 1.6 %convolution_convert_fusion.6 = bf16[24,256]{1,0:T(8,128)(2,1)S(1)} fusion(bf16[2048,256]{1,0:T(8,128)(2,1)} %param.27, bf16[24,2048]{1,0:T(8,128)(2,1)} %param.23, f32[2048]{0:T(1024)S(1)} %convert_element_type.87, f32[24]{0:T(128)S(1)} %add_rsqrt_fusion.4), kind=kOutput, calls=%fused_computation.24 | convolution fusion | flops 25368576 | bytes 1167456 | tf_op jit(solution)/shard_map/dot_general | solution.py:101
  7.3 0.1 multiply_reduce_fusion.3
  7.4 0.1 copy.38
  7.5 1.6 %convolution_convert_fusion.5 = bf16[24,256]{1,0:T(8,128)(2,1)S(1)} fusion(bf16[2048,256]{1,0:T(8,128)(2,1)} %param.28, bf16[24,2048]{1,0:T(8,128)(2,1)} %param.23, f32[2048]{0:T(1024)S(1)} %convert_element_type.87, f32[24]{0:T(128)S(1)} %add_rsqrt_fusion.4), kind=kOutput, calls=%fused_computation.23 | convolution fusion | flops 25368576 | bytes 1167456 | tf_op jit(solution)/shard_map/dot_general | solution.py:101
  9.1 0.3 convolution_convert_fusion.4
  9.4 0.0 copy-start.1
  9.4 0.1 multiply_reduce_fusion.2
  9.6 0.1 broadcast_multiply_fusion.1
  9.7 2.6 %fusion = f32[24,2,1,128]{3,2,1,0:T(1,128)S(1)} fusion(f32[24,2,128,1]{2,3,1,0:T(1,128)S(1)} %bitcast.63, f32[24,2,128,128]{3,2,1,0:T(8,128)} %param.24, f32[24,2]{1,0:T(8,128)S(1)} %copy.38), kind=kOutput, calls=%fused_computation.2 | convolution fusion | flops 2359296 | bytes 3195072 | tf_op jit(solution)/shard_map/shkv,shk->shv/dot_general | solution.py:45
  12.4 1.1 %multiply_add_fusion = f32[24,2,128,128]{3,2,1,0:T(8,128)S(1)} fusion(f32[24,2,128,128]{3,2,1,0:T(8,128)S(1)} %copy-done.1, f32[24,2,128]{2,1,0:T(2,128)S(1)} %fusion.47, f32[24,2,128]{2,1,0:T(2,128)S(1)} %get-tuple-element.6, f32[24,2]{1,0:T(8,128)S(1)} %copy.38), kind=kLoop, calls=%fused_computation.1 | loop fusion | flops 2359296 | bytes 6340800 | tf_op jit(solution)/shard_map/add | solution.py:49
  13.5 0.0 copy-start.2
  13.5 0.0 copy-start.5
  13.5 0.1 multiply_multiply_fusion
  13.6 1.5 %copy-done.2 = f32[24,2,128,128]{3,2,1,0:T(8,128)} copy-done((f32[24,2,128,128]{3,2,1,0:T(8,128)}, f32[24,2,128,128]{3,2,1,0:T(8,128)S(1)}, u32[]{:S(2)}) %copy-start.2) | copy-done | bytes 3145752
  15.2 0.5 fusion.76
  15.7 0.1 multiply_reduce_fusion.1
  15.8 0.0 copy-done.5
  15.8 0.3 convolution_convert_fusion.3
  16.1 0.0 copy-done.11
  16.2 0.1 fusion.50
  16.3 0.2 copy-done.6
  16.5 0.2 convolution_convert_fusion.2
  16.7 0.0 copy-start.9
  16.8 9.3 %all-gather = bf16[96,2048]{1,0:T(8,128)(2,1)S(1)} all-gather(bf16[24,2048]{1,0:T(8,128)(2,1)S(1)} %convolution_convert_fusion.2), channel_id=2, replica_groups=mesh['ep'=64,'tp'=4] {'tp'}, dimensions={0}, use_global_device_ids=true | all-gather | bytes 491520 | tf_op jit(solution)/shard_map/all_gather | solution.py:12
  26.1 0.1 fusion.35
  26.3 0.0 copy-done.10
  26.3 0.1 copy.40
  26.4 0.1 eq.52
  26.5 0.2 convert_reduce_fusion.2
  26.7 0.1 reduce_sum.101
  26.8 0.1 copy.46
  26.9 0.1 fusion.41
  27.0 0.4 convolution_convert_fusion.1
  27.4 1.1 %reshape.270 = bf16[64,2,2048]{2,1,0:T(2,128)(2,1)} reshape(bf16[128,2048]{1,0:T(8,128)(2,1)S(1)} %convolution_convert_fusion.1) | data formatting | bytes 1048576 | tf_op jit(solution)/shard_map/reshape | solution.py:148
  28.5 12.6 %all-to-all-start = ((bf16[64,2,2048]{2,1,0:T(2,128)(2,1)}), bf16[64,2,2048]{2,1,0:T(2,128)(2,1)S(1)}, u32[]{:S(2)}, u32[]{:S(2)}) async-start(bf16[64,2,2048]{2,1,0:T(2,128)(2,1)} %reshape.270), calls=%async_computation | async-start | bytes 1048576 | tf_op jit(solution)/shard_map/all_to_all | solution.py:149
  41.1 0.1 reshape.274
  41.2 0.0 copy-done.7
  41.2 0.1 copy.43
  41.3 17.3 %all-to-all-done = bf16[64,2,2048]{2,1,0:T(2,128)(2,1)S(1)} async-done(((bf16[64,2,2048]{2,1,0:T(2,128)(2,1)}), bf16[64,2,2048]{2,1,0:T(2,128)(2,1)S(1)}, u32[]{:S(2)}, u32[]{:S(2)}) %all-to-all-start) | async-done | bytes 524320 | tf_op jit(solution)/shard_map/all_to_all | solution.py:149
  58.6 0.2 reshape.271
  58.8 2.7 %fusion.7 = f32[128,512]{1,0:T(8,128)} fusion(bf16[128,2048]{1,0:T(8,128)(2,1)S(1)} %reshape.271, bf16[1,2048,512]{2,1,0:T(8,128)(2,1)} %param.41), kind=kOutput, calls=%fused_computation.13 | convolution fusion | flops 268435456 | bytes 2883584 | tf_op jit(solution)/shard_map/dot_general | solution.py:60
  61.6 2.4 %convolution_convert_fusion = bf16[128,2048]{1,0:T(8,128)(2,1)S(1)} fusion(bf16[1,512,2048]{2,1,0:T(8,128)(2,1)S(1)} %copy-done, bf16[128,2048]{1,0:T(8,128)(2,1)S(1)} %reshape.271, bf16[1,2048,512]{2,1,0:T(8,128)(2,1)} %param.42, f32[128,512]{1,0:T(8,128)} %fusion.7), kind=kOutput, calls=%fused_computation.4 | convolution fusion | flops 537526272 | bytes 5505024 | tf_op jit(solution)/shard_map/dot_general | solution.py:63
  64.0 1.1 %reshape.272 = bf16[64,2,2048]{2,1,0:T(2,128)(2,1)} reshape(bf16[128,2048]{1,0:T(8,128)(2,1)S(1)} %convolution_convert_fusion) | data formatting | bytes 1048576 | tf_op jit(solution)/shard_map/reshape | solution.py:154
  65.1 7.0 %all-to-all-start.1 = ((bf16[64,2,2048]{2,1,0:T(2,128)(2,1)}), bf16[64,2,2048]{2,1,0:T(2,128)(2,1)S(1)}, u32[]{:S(2)}, u32[]{:S(2)}) async-start(bf16[64,2,2048]{2,1,0:T(2,128)(2,1)} %reshape.272), calls=%async_computation.1 | async-start | bytes 1048576 | tf_op jit(solution)/shard_map/all_to_all | solution.py:153
  72.2 0.1 multiply_select_fusion
  72.2 0.2 fusion.25
  72.5 2.0 %fusion.65 = f32[24,512]{1,0:T(8,128)S(1)} fusion(bf16[2048,512]{1,0:T(8,128)(2,1)} %param.38, bf16[24,2048]{1,0:T(8,128)(2,1)S(1)} %get-tuple-element.3, f32[2048]{0:T(1024)S(1)} %convert_element_type.101, f32[24]{0:T(128)S(1)} %add_rsqrt_fusion.3), kind=kOutput, calls=%fused_computation.115 | convolution fusion | flops 50528256 | bytes 2252896 | tf_op jit(solution)/shard_map/dot_general | solution.py:125
  74.5 14.3 %all-to-all-done.1 = bf16[64,2,2048]{2,1,0:T(2,128)(2,1)S(1)} async-done(((bf16[64,2,2048]{2,1,0:T(2,128)(2,1)}), bf16[64,2,2048]{2,1,0:T(2,128)(2,1)S(1)}, u32[]{:S(2)}, u32[]{:S(2)}) %all-to-all-start.1) | async-done | bytes 524320 | tf_op jit(solution)/shard_map/all_to_all | solution.py:153
  88.8 0.2 reshape.273
  89.0 1.0 gather_fusion
  89.9 1.3 %reshape.283 = f32[24,6,2048]{2,1,0:T(8,128)} reshape(bf16[144,2048]{1,0:T(8,128)(2,1)S(1)} %gather_fusion) | data formatting | bytes 1769472 | tf_op jit(solution)/shard_map/convert_element_type | solution.py:157
  91.2 2.0 %multiply_reduce_fusion = f32[24,2048]{1,0:T(8,128)S(1)} fusion(f32[24,6,2048]{2,1,0:T(8,128)} %reshape.283, f32[24,6]{1,0:T(8,128)S(1)} %multiply_select_fusion), kind=kLoop, calls=%fused_computation.15 | loop fusion | flops 540672 | bytes 1376832 | tf_op jit(solution)/shard_map/reduce_sum | solution.py:161
  93.2 3.0 %fusion.3 = bf16[24,2048]{1,0:T(8,128)(2,1)S(1)} fusion(f32[24,2048]{1,0:T(8,128)S(1)} %multiply_reduce_fusion, bf16[512,2048]{1,0:T(8,128)(2,1)} %param.40, bf16[2048,512]{1,0:T(8,128)(2,1)} %param.39, f32[24]{0:T(128)S(1)} %fusion.25, f32[24,512]{1,0:T(8,128)S(1)} %fusion.65, bf16[24,2048]{1,0:T(8,128)(2,1)S(1)} %get-tuple-element.3, ...), kind=kOutput, calls=%fused_computation.8 | convolution fusion | flops 101081088 | bytes 4645056 | tf_op jit(solution)/shard_map/dot_general | solution.py:128
  96.3 12.6 %all_to_all.15 = bf16[4,24,2048]{2,1,0:T(8,128)(2,1)S(1)} all-to-all(bf16[4,24,2048]{2,1,0:T(8,128)(2,1)S(1)} %broadcast_in_dim.7), channel_id=1, replica_groups=mesh['ep'=64,'tp'=4] {'tp'}, dimensions={0} | all-to-all | bytes 786432 | tf_op jit(solution)/shard_map/all_to_all | solution.py:18
  109.0 0.7 fusion.38
  (32 shorter events, 0.4 us)
Async XLA Ops:
  0.6 61.0 %copy-start = (bf16[1,512,2048]{2,1,0:T(8,128)(2,1)S(1)}, bf16[1,512,2048]{2,1,0:T(8,128)(2,1)}, u32[]{:S(2)}) copy-start(bf16[1,512,2048]{2,1,0:T(8,128)(2,1)} %param.43) | copy-start | bytes 6291460
  0.6 8.4 %copy-start.3 = (bf16[24,2048]{1,0:T(8,128)(2,1)S(1)}, bf16[24,2048]{1,0:T(8,128)(2,1)}, u32[]{:S(2)}) copy-start(bf16[24,2048]{1,0:T(8,128)(2,1)} %param.23) | copy-start | bytes 294916
  0.7 8.4 %copy-start.4 = (bf16[2048,256]{1,0:T(8,128)(2,1)S(1)}, bf16[2048,256]{1,0:T(8,128)(2,1)}, u32[]{:S(2)}) copy-start(bf16[2048,256]{1,0:T(8,128)(2,1)} %param.26) | copy-start | bytes 3145732
  9.4 2.9 %copy-start.1 = (f32[24,2,128,128]{3,2,1,0:T(8,128)S(1)}, f32[24,2,128,128]{3,2,1,0:T(8,128)}, u32[]{:S(2)}) copy-start(f32[24,2,128,128]{3,2,1,0:T(8,128)} %param.24) | copy-start | bytes 9437188
  13.5 1.7 %copy-start.2 = (f32[24,2,128,128]{3,2,1,0:T(8,128)}, f32[24,2,128,128]{3,2,1,0:T(8,128)S(1)}, u32[]{:S(2)}) copy-start(f32[24,2,128,128]{3,2,1,0:T(8,128)S(1)} %multiply_add_fusion) | copy-start | bytes 9437188
  13.5 2.3 %copy-start.5 = (bf16[2048,256]{1,0:T(8,128)(2,1)S(1)}, bf16[2048,256]{1,0:T(8,128)(2,1)}, u32[]{:S(2)}) copy-start(bf16[2048,256]{1,0:T(8,128)(2,1)} %param.29) | copy-start | bytes 3145732
  15.2 1.0 copy-start.11
  15.2 1.3 %copy-start.6 = (bf16[256,2048]{1,0:T(8,128)(2,1)S(1)}, bf16[256,2048]{1,0:T(8,128)(2,1)}, u32[]{:S(2)}) copy-start(bf16[256,2048]{1,0:T(8,128)(2,1)} %param.35) | copy-start | bytes 3145732
  15.7 10.6 %copy-start.10 = (s32[24,6]{0,1:T(8,128)S(1)}, s32[24,6]{0,1:T(8,128)}, u32[]{:S(2)}) copy-start(s32[24,6]{0,1:T(8,128)} %param.44) | copy-start | bytes 1732
  15.7 11.3 %copy-start.8 = (bf16[2048]{0:T(1024)(128)(2,1)S(1)}, bf16[2048]{0:T(1024)(128)(2,1)}, u32[]{:S(2)}) copy-start(bf16[2048]{0:T(1024)(128)(2,1)} %param.36) | copy-start | bytes 12292
  16.7 24.5 %copy-start.7 = (f32[24,6]{0,1:T(8,128)S(1)}, f32[24,6]{0,1:T(8,128)}, u32[]{:S(2)}) copy-start(f32[24,6]{0,1:T(8,128)} %param.45) | copy-start | bytes 1732
  16.7 24.6 %copy-start.9 = (bf16[2048]{0:T(1024)(128)(2,1)S(1)}, bf16[2048]{0:T(1024)(128)(2,1)}, u32[]{:S(2)}) copy-start(bf16[2048]{0:T(1024)(128)(2,1)} %param.37) | copy-start | bytes 12292
  28.5 30.1 %all-to-all-start = ((bf16[64,2,2048]{2,1,0:T(2,128)(2,1)}), bf16[64,2,2048]{2,1,0:T(2,128)(2,1)S(1)}, u32[]{:S(2)}, u32[]{:S(2)}) async-start(bf16[64,2,2048]{2,1,0:T(2,128)(2,1)} %reshape.270), calls=%async_computation | async-start | bytes 1048576 | tf_op jit(solution)/shard_map/all_to_all | solution.py:149
  65.1 23.6 %all-to-all-start.1 = ((bf16[64,2,2048]{2,1,0:T(2,128)(2,1)}), bf16[64,2,2048]{2,1,0:T(2,128)(2,1)S(1)}, u32[]{:S(2)}, u32[]{:S(2)}) async-start(bf16[64,2,2048]{2,1,0:T(2,128)(2,1)} %reshape.272), calls=%async_computation.1 | async-start | bytes 1048576 | tf_op jit(solution)/shard_map/all_to_all | solution.py:153
where the time goes:
time: 110 us
  waiting for transfers between devices  31.6 us (29%)
  blocking collectives  21.9 us (20%)
  matrix products  20.2 us (18%)
  starting transfers between devices  19.6 us (18%)
  other arithmetic  7.73 us (7%)
  local copies, waits for them, and re-layouts  7.62 us (7%)
    all_to_all x1, waiting for transfers between devices, shards(): lax.all_to_all(outgoing, 'ep', split_axis=0, concat_axis=0, tiled=True)  17.3 us
    all_to_all x1, waiting for transfers between devices, shards(): lax.all_to_all(result.reshape(arrived.shape), 'ep', split_axis=0, concat_...  14.3 us
    all_to_all x1, blocking collectives, sent_to_all(): lax.all_to_all(jnp.broadcast_to(x[None], (devices, *x.shape)), axis, 0, 0...  12.6 us
    all_to_all x1, starting transfers between devices, shards(): lax.all_to_all(outgoing, 'ep', split_axis=0, concat_axis=0, tiled=True)  12.6 us
    all_gather x1, blocking collectives, over_pieces(): pieces = lax.all_gather(x, axis).astype(jnp.float32)  9.31 us
    all_to_all x1, starting transfers between devices, shards(): lax.all_to_all(result.reshape(arrived.shape), 'ep', split_axis=0, concat_...  6.97 us
    dot_general x4, matrix products, project(): product = jnp.dot(normed, weight, preferred_element_type=jnp.float32)  3.74 us
    dot_general x1, matrix products, shards(): jnp.dot(dense_hidden, dense_down_weight, preferred_element_type=jnp.float32)  3.02 us
  transfers between devices with their start and end apart: 2, of which 2 were waited for; matrix products, arithmetic and copies ran while one was open for 2% of the time, Pallas kernels for 0%

commit v1 on v0

v1 whole, which is shorter than its diff:
```python
import functools

import jax
import jax.numpy as jnp
from jax import lax
from jax.experimental import pallas as pl
from jax.experimental.pallas import tpu as pltpu
from jax.sharding import PartitionSpec as P

NORM_EPS = 1e-06
UNIT_EPS = 1e-06
ROUTED_SCALE = 2.5
MESH = pl.DeviceIdType.MESH
F32 = jnp.float32
BF16 = jnp.bfloat16
VMEM = pltpu.VMEM
Q = 4
PAD = 32
CAP = 2


def silu(x):
    return x * jax.nn.sigmoid(x)


def dot(a, b):
    return jnp.dot(a, b, preferred_element_type=F32)


def unit_rows(x):
    return x * lax.rsqrt(jnp.sum(x * x, axis=-1, keepdims=True) + UNIT_EPS)


def rms_inverse(total, width):
    return lax.rsqrt(total * (1.0 / width) + NORM_EPS)


def turned(x):
    rows, width = x.shape
    return jnp.transpose(jnp.concatenate([x, jnp.zeros((width - rows, width), F32)], axis=0))


def mixer(
    tokens, first_gain, beta_t, decay_t, rate, bias, head_gain,
    query_w, key_w, value_w, gate_w, out_w, state,
    mixed, new_state,
    weights, out_weights, held, read, in_sem, state_sem, back_sem,
    chunk,
):
    rows, width = tokens.shape
    heads, size = held.shape[1], held.shape[2]
    chunks = rows // chunk
    loads = [
        pltpu.make_async_copy(w, weights.at[i], in_sem.at[i])
        for i, w in enumerate((key_w, value_w, query_w, gate_w))
    ]
    loads.append(pltpu.make_async_copy(out_w, out_weights, in_sem.at[4]))
    pieces = [
        pltpu.make_async_copy(
            state.at[pl.ds(c * chunk, chunk)], held.at[pl.ds(c * chunk, chunk)], state_sem.at[c]
        )
        for c in range(chunks)
    ]
    for copy in loads[:4] + pieces + loads[4:]:
        copy.start()

    x = tokens[...].astype(F32)
    total = jnp.sum(x * x, axis=-1, keepdims=True)
    normed = (x * rms_inverse(total, width) * first_gain[...].astype(F32)).astype(BF16)

    def across(w):
        return lax.dot_general(normed, w[...], (((1,), (1,)), ((), ())), preferred_element_type=F32)

    beta_all = jax.nn.sigmoid(across(beta_t))
    decay_in = across(decay_t) + bias[...]
    softplus = jnp.maximum(decay_in, 0.0) + jnp.log1p(jnp.exp(-jnp.abs(decay_in)))
    decay_all = jnp.exp(-rate[...] * softplus)
    head_at = lax.broadcasted_iota(jnp.int32, beta_all.shape, 1)
    first_head = lax.axis_index("tp") * heads

    def of_head(values, h):
        column = jnp.sum(
            jnp.where(head_at == first_head + h, values, 0.0), axis=1, keepdims=True
        )
        return jnp.broadcast_to(column, (rows, size))

    def project(i):
        loads[i].wait()
        return dot(normed, weights[i]).astype(BF16).astype(F32)

    key_raw, value_raw, query_raw, gate_raw = [project(i) for i in range(4)]
    keys, queries, values, betas, decays = [], [], [], [], []
    for h in range(heads):
        part = slice(h * size, (h + 1) * size)
        keys.append(turned(unit_rows(silu(key_raw[:, part]))))
        queries.append(turned(unit_rows(silu(query_raw[:, part])) * size ** (-0.5)))
        values.append(silu(value_raw[:, part]))
        betas.append(of_head(beta_all, h))
        decays.append(of_head(decay_all, h))
    backs = []
    for c in range(chunks):
        pieces[c].wait()
        for s in range(c * chunk, (c + 1) * chunk):
            for h in range(heads):
                key = jnp.broadcast_to(keys[h][:, s : s + 1], (size, size))
                query = jnp.broadcast_to(queries[h][:, s : s + 1], (size, size))
                decayed = held[s, h] * decays[h][s : s + 1, :]
                predicted = jnp.sum(decayed * key, axis=0, keepdims=True)
                change = betas[h][s : s + 1, :] * (values[h][s : s + 1, :] - predicted)
                new = decayed + key * change
                held[s, h] = new
                read[s : s + 1, h * size : (h + 1) * size] = jnp.sum(
                    new * query, axis=0, keepdims=True
                )
        back = pltpu.make_async_copy(
            held.at[pl.ds(c * chunk, chunk)], new_state.at[pl.ds(c * chunk, chunk)], back_sem.at[c]
        )
        back.start()
        backs.append(back)
    gated = []
    for h in range(heads):
        part = slice(h * size, (h + 1) * size)
        r = read[:, part]
        inverse = rms_inverse(jnp.sum(r * r, axis=-1, keepdims=True), size)
        gated.append(
            (r * inverse * head_gain[...].astype(F32) * silu(gate_raw[:, part])).astype(BF16)
        )
    gated = jnp.concatenate(gated, axis=1)
    loads[4].wait()
    columns = width // Q
    for q in range(Q):
        mixed[q] = dot(gated, out_weights[:, q * columns : (q + 1) * columns]).astype(BF16)
    return backs


def mixer_kernel(*refs, chunk):
    for back in mixer(*refs, chunk=chunk):
        back.wait()


def spread(table, fill):
    k, tokens = table.shape
    side = jnp.full((k, PAD - tokens), fill, table.dtype)
    return jnp.concatenate([table, side] * Q, axis=1)


def exchange_kernel(
    mixed, tokens, gain, blend, ids, scales,
    dense_gate, dense_up, dense_down, expert_gate, expert_up, expert_down,
    new_tokens,
    w_gate, w_up, w_down, e_gate, e_up, e_down,
    pair_in, chip_sum, chip_in, pair_in2, part2, chip_sum2, chip_in2,
    rows_mid, full_mid, out_box, in_box, wide, back_box, got_box, combined,
    w_sem, pair_sem, chip_send, chip_recv, go_send, go_recv, back_send, back_recv,
):
    groups = lax.axis_size("ep")
    ep, tp = lax.axis_index("ep"), lax.axis_index("tp")
    core = lax.rem(tp, 2)
    partner = tp + 1 - 2 * core
    others = lax.rem(tp - core + 2, 4)
    count, width = tokens.shape
    columns = width // Q
    hidden_size = w_gate.shape[1]

    def place(i):
        return lax.rem(ep + i, groups), lax.rem(tp + 2 * lax.rem(i, 2), 4)

    loads = [
        pltpu.make_async_copy(src, dst, w_sem.at[n])
        for n, (src, dst) in enumerate(
            (
                (dense_gate, w_gate),
                (dense_up, w_up),
                (dense_down, w_down),
                (expert_gate.at[0], e_gate),
                (expert_up.at[0], e_up),
                (expert_down.at[0], e_down),
            )
        )
    ]
    for load in loads:
        load.start()

    barrier = pltpu.get_barrier_semaphore()

    def greet(i, carry):
        pl.semaphore_signal(barrier, inc=1, device_id=place(i), device_id_type=MESH)
        return carry

    lax.fori_loop(1, groups, greet, 0)
    for i in range(1, 4):
        pl.semaphore_signal(
            barrier, inc=1, device_id=(ep, lax.rem(tp + i, 4)), device_id_type=MESH
        )
    pl.semaphore_wait(barrier, groups - 1 + 3)

    def over_tp(part, pair_buffer, total, chip_buffer, n, between):
        pair = pltpu.make_async_remote_copy(
            src_ref=part, dst_ref=pair_buffer, send_sem=pair_sem.at[2 * n], recv_sem=pair_sem.at[2 * n + 1],
            device_id=(ep, partner), device_id_type=MESH,
        )
        pair.start()
        between()
        pair.wait()
        total[...] = (part[...].astype(F32) + pair_buffer[...].astype(F32)).astype(BF16)
        half = pl.ds(core * (Q // 2), Q // 2)
        sends = []
        for c in range(2):
            sends.append(
                pltpu.make_async_remote_copy(
                    src_ref=total.at[half], dst_ref=chip_buffer.at[half],
                    send_sem=chip_send.at[n, c], recv_sem=chip_recv.at[n, core],
                    device_id=(ep, others + c), device_id_type=MESH,
                )
            )
            sends[-1].start()
        return sends

    def finish(sends, total, chip_buffer, n):
        for c in range(2):
            part = pl.ds(c * (Q // 2), Q // 2)
            pltpu.make_async_remote_copy(
                src_ref=total.at[part], dst_ref=chip_buffer.at[part],
                send_sem=chip_send.at[n, c], recv_sem=chip_recv.at[n, c],
                device_id=(ep, others), device_id_type=MESH,
            ).wait_recv()
        for send in sends:
            send.wait_send()

    slots = groups * CAP * Q
    lanes = Q * PAD
    tables = {}

    def build_tables():
        ids_c = spread(ids[...], -1)
        raw = scales[...]
        scale_c = spread(raw / jnp.sum(raw, axis=0, keepdims=True) * ROUTED_SCALE, 0.0)
        row = lax.broadcasted_iota(jnp.int32, (slots, 1), 0)
        offset = row // (CAP * Q)
        expert = lax.rem(ep + offset, groups) * 4 + lax.rem(tp + 2 * lax.rem(offset, 2), 4)
        named = jnp.zeros((slots, lanes), F32)
        weight = jnp.zeros((slots, lanes), F32)
        for k in range(ids.shape[0]):
            hit = ids_c[k : k + 1, :] == expert
            named = jnp.where(hit, 1.0, named)
            weight = jnp.where(hit, scale_c[k : k + 1, :], weight)
        a = lax.broadcasted_iota(jnp.int32, (lanes, lanes), 0)
        b = lax.broadcasted_iota(jnp.int32, (lanes, lanes), 1)
        earlier = ((a // PAD == b // PAD) & (a < b)).astype(F32).astype(BF16)
        rank = dot(named.astype(BF16), earlier)
        slot = lax.rem(row // Q, CAP).astype(F32)
        piece = lax.rem(row, Q)
        at = lax.broadcasted_iota(jnp.int32, (slots, lanes), 1) // PAD
        taken = (named > 0.5) & (rank == slot) & (piece == at)
        tables["pick"] = jnp.where(taken, 1.0, 0.0).astype(BF16)
        tables["weight"] = jnp.transpose(jnp.where(taken, weight, 0.0))

    sends = over_tp(mixed, pair_in, chip_sum, chip_in, 0, build_tables)
    rows_mid[...] = jnp.zeros_like(rows_mid)
    finish(sends, chip_sum, chip_in, 0)

    residual = []
    squares = jnp.zeros((count, 1), F32)
    for q in range(Q):
        part = slice(q * columns, (q + 1) * columns)
        mix = chip_sum[q].astype(F32) + chip_in[q].astype(F32)
        res = (tokens[:, part].astype(F32) + mix).astype(BF16).astype(F32)
        residual.append(res)
        squares += jnp.sum(res * res, axis=-1, keepdims=True)
    inverse = rms_inverse(squares, width)
    blended = jnp.zeros((count, 1), F32)
    for q in range(Q):
        part = slice(q * columns, (q + 1) * columns)
        mid = (residual[q] * inverse * gain[:, part].astype(F32)).astype(BF16)
        rows_mid[q * PAD : q * PAD + count, :] = mid
        full_mid[:, part] = mid
        blended += jnp.sum(
            mid.astype(F32) * blend[:, part].astype(F32), axis=-1, keepdims=True
        )
    blend_gate = jax.nn.sigmoid(blended)
    outgoing = dot(tables["pick"], rows_mid[...]).astype(BF16)
    out_box[...] = outgoing.reshape(out_box.shape)

    def go(i):
        return pltpu.make_async_remote_copy(
            src_ref=out_box.at[i], dst_ref=in_box.at[i], send_sem=go_send, recv_sem=go_recv,
            device_id=place(i), device_id_type=MESH,
        )

    def go_start(i, carry):
        go(i).start()
        return carry

    lax.fori_loop(1, groups, go_start, 0)
    in_box[0] = out_box[0]

    for n in range(3):
        loads[n].wait()
    mid = full_mid[...]
    dense_hidden = (silu(dot(mid, w_gate[...])) * dot(mid, w_up[...])).astype(BF16)
    for q in range(Q):
        part = slice(q * columns, (q + 1) * columns)
        combined[q] = blend_gate * dot(dense_hidden, w_down[:, part])
    for n in range(3, 6):
        loads[n].wait()

    rest = pl.ds(1, groups - 1)
    arrived = pltpu.make_async_remote_copy(
        src_ref=out_box.at[rest], dst_ref=in_box.at[rest], send_sem=go_send, recv_sem=go_recv,
        device_id=(ep, partner), device_id_type=MESH,
    )
    arrived.wait_recv()
    tiles = columns // 128
    flat = in_box[...].reshape(slots, columns).astype(F32)
    for t in range(tiles):
        wide[t] = flat[:, t * 128 : (t + 1) * 128]
    count_slots = groups * CAP
    gate_part = jnp.zeros((count_slots, hidden_size), F32)
    up_part = jnp.zeros((count_slots, hidden_size), F32)
    for q in range(Q):
        part = slice(q * columns, (q + 1) * columns)
        block = jnp.concatenate(
            [wide[t, pl.ds(q, count_slots, stride=Q), :] for t in range(tiles)], axis=1
        ).astype(BF16)
        gate_part += dot(block, e_gate[part, :])
        up_part += dot(block, e_up[part, :])
    hidden = (silu(gate_part) * up_part).astype(BF16)
    for q in range(Q):
        part = slice(q * columns, (q + 1) * columns)
        down = dot(hidden, e_down[:, part])
        for t in range(tiles):
            wide[t, pl.ds(q, count_slots, stride=Q), :] = down[:, t * 128 : (t + 1) * 128]
    back = jnp.concatenate([wide[t] for t in range(tiles)], axis=1).astype(BF16)
    back_box[...] = back.reshape(back_box.shape)

    def back_start(i, carry):
        group, lane = place(groups - i)
        pltpu.make_async_remote_copy(
            src_ref=back_box.at[i], dst_ref=got_box.at[i], send_sem=back_send, recv_sem=back_recv,
            device_id=(group, lane), device_id_type=MESH,
        ).start()
        return carry

    lax.fori_loop(1, groups, back_start, 0)
    got_box[0] = back_box[0]
    weight = tables["weight"]
    high = weight.astype(BF16)
    low = (weight - high.astype(F32)).astype(BF16)
    arrived.wait_send()
    returned = pltpu.make_async_remote_copy(
        src_ref=back_box.at[rest], dst_ref=got_box.at[rest], send_sem=back_send, recv_sem=back_recv,
        device_id=(ep, partner), device_id_type=MESH,
    )
    returned.wait_recv()
    results = got_box[...].reshape(slots, columns)
    routed = dot(high, results) + dot(low, results)
    for q in range(Q):
        part2[q] = (combined[q] + routed[q * PAD : q * PAD + count, :]).astype(BF16)

    sends = over_tp(part2, pair_in2, chip_sum2, chip_in2, 1, lambda: None)
    finish(sends, chip_sum2, chip_in2, 1)
    for q in range(Q):
        part = slice(q * columns, (q + 1) * columns)
        more = chip_sum2[q].astype(F32) + chip_in2[q].astype(F32)
        new_tokens[:, part] = (residual[q] + more).astype(BF16)
    returned.wait_send()


def shards(
    tokens, delta_state, first_gain, query_weight, key_weight, value_weight, outgate_weight,
    beta_weight, decay_weight, decay_rate, decay_bias, head_gain, out_weight, second_gain,
    blend_weight, dense_gate_weight, dense_up_weight, dense_down_weight,
    expert_gate, expert_up, expert_down, route_ids, route_weights,
):
    count, width = tokens.shape
    heads, size = delta_state.shape[1], delta_state.shape[2]
    groups = lax.axis_size("ep")
    columns = width // Q
    hidden = dense_gate_weight.shape[1]
    expert_hidden = expert_gate.shape[2]
    anywhere = pl.BlockSpec(memory_space=pl.ANY)
    near = pl.BlockSpec(memory_space=VMEM)
    chunk = 4
    mixed, new_state = pl.pallas_call(
        functools.partial(mixer_kernel, chunk=chunk),
        out_shape=(
            jax.ShapeDtypeStruct((Q, count, columns), BF16),
            jax.ShapeDtypeStruct(delta_state.shape, F32),
        ),
        in_specs=[near] * 7 + [anywhere] * 6,
        out_specs=(near, anywhere),
        scratch_shapes=[
            VMEM((4, width, heads * size), BF16),
            VMEM((heads * size, width), BF16),
            VMEM(delta_state.shape, F32),
            VMEM((count, heads * size), F32),
            pltpu.SemaphoreType.DMA((5,)),
            pltpu.SemaphoreType.DMA((count // chunk,)),
            pltpu.SemaphoreType.DMA((count // chunk,)),
        ],
        compiler_params=pltpu.CompilerParams(vmem_limit_bytes=32 << 20),
        name="mixer",
    )(
        tokens, first_gain[None], beta_weight.T, decay_weight.T, decay_rate[None],
        decay_bias[None], head_gain[None],
        query_weight, key_weight, value_weight, outgate_weight, out_weight, delta_state,
    )
    wire = VMEM((Q, count, columns), BF16)
    box = VMEM((groups, CAP * Q, columns), BF16)
    new_tokens = pl.pallas_call(
        exchange_kernel,
        out_shape=jax.ShapeDtypeStruct((count, width), BF16),
        in_specs=[near] * 6 + [anywhere] * 6,
        out_specs=near,
        scratch_shapes=[
            VMEM((width, hidden), BF16),
            VMEM((width, hidden), BF16),
            VMEM((hidden, width), BF16),
            VMEM((width, expert_hidden), BF16),
            VMEM((width, expert_hidden), BF16),
            VMEM((expert_hidden, width), BF16),
            wire, wire, wire, wire, wire, wire, wire,
            VMEM((Q * PAD, columns), BF16),
            VMEM((count, width), BF16),
            box,
            box,
            VMEM((columns // 128, groups * CAP * Q, 128), F32),
            box,
            box,
            VMEM((Q, count, columns), F32),
            pltpu.SemaphoreType.DMA((6,)),
            pltpu.SemaphoreType.DMA((4,)),
            pltpu.SemaphoreType.DMA((2, 2)),
            pltpu.SemaphoreType.DMA((2, 2)),
            pltpu.SemaphoreType.DMA,
            pltpu.SemaphoreType.DMA,
            pltpu.SemaphoreType.DMA,
            pltpu.SemaphoreType.DMA,
        ],
        compiler_params=pltpu.CompilerParams(
            collective_id=0, has_side_effects=True, vmem_limit_bytes=48 << 20
        ),
        name="exchange",
    )(
        mixed, tokens, second_gain[None], blend_weight[None], route_ids.T, route_weights.T,
        dense_gate_weight, dense_up_weight, dense_down_weight,
        expert_gate, expert_up, expert_down,
    )
    return (new_tokens, new_state)


def solution(mesh):
    placed = (
        P("ep", None),
        P("ep", "tp", None, None),
        P(),
        P(None, "tp"),
        P(None, "tp"),
        P(None, "tp"),
        P(None, "tp"),
        P(),
        P(),
        P(),
        P(),
        P(),
        P("tp", None),
        P(),
        P(),
        P(None, "tp"),
        P(None, "tp"),
        P("tp", None),
        P(("ep", "tp"), None, None),
        P(("ep", "tp"), None, None),
        P(("ep", "tp"), None, None),
        P("ep", None),
        P("ep", None),
    )
    return jax.shard_map(
        shards,
        mesh=mesh,
        in_specs=placed,
        out_specs=(P("ep", None), P("ep", "tp", None, None)),
        check_vma=False,
    )
```

time: 110 us -> 79 us (0.72)
  Pallas kernels: 0 us -> 62.5 us
  waiting for transfers between devices: 31.6 us -> 0 us
  blocking collectives: 21.9 us -> 0 us
  matrix products: 20.2 us -> 0 us
  starting transfers between devices: 19.6 us -> 0 us
  other arithmetic: 7.73 us -> 0 us
  local copies, waits for them, and re-layouts: 7.62 us -> 15.1 us
    pallas_call x0 -> x2, Pallas kernels: none -> 62.5 us  [the longest x1 57 us: shards(): pl.pallas_call(exchange_kernel, out_shape=jax.ShapeDtypeStruct((count, wi...]
    all_to_all x2 -> x0, waiting for transfers between devices: 31.6 us -> none  [the longest x1 17.3 us: shards(): lax.all_to_all(outgoing, 'ep', split_axis=0, concat_axis=0, tiled=True)]
    dot_general x15 -> x0, matrix products: 20.2 us -> none  [the longest x4 3.74 us: project(): product = jnp.dot(normed, weight, preferred_element_type=jnp.float32)]
    all_to_all x2 -> x0, starting transfers between devices: 19.6 us -> none  [the longest x1 12.6 us: shards(): lax.all_to_all(outgoing, 'ep', split_axis=0, concat_axis=0, tiled=True)]
    all_to_all x1 -> x0, blocking collectives: 12.6 us -> none  [sent_to_all(): lax.all_to_all(jnp.broadcast_to(x[None], (devices, *x.shape)), axis, 0, 0...]
    unnamed x27 -> x35, local copies, waits for them, and re-layouts: 2 us -> 13 us
    all_gather x1 -> x0, blocking collectives: 9.31 us -> none  [over_pieces(): pieces = lax.all_gather(x, axis).astype(jnp.float32)]
    reduce_sum x10 -> x0, other arithmetic: 3.84 us -> none  [the longest x1 1.97 us: shards(): routed_part = jnp.sum(kept_scale[:, :, None] * picked, axis=1)]
  transfers between devices with their start and end apart: 2 -> 0, of which waited for: 2 -> 0; matrix products, arithmetic and copies ran while one was open for 2% -> 0% of each run, Pallas kernels for 0% -> 0%
where the time goes in v1:
time: 79 us; the launch traced here: 78.4 us
  Pallas kernels  62.5 us (79%)
  local copies, waits for them, and re-layouts  15.1 us (19%)
    pallas_call x1, Pallas kernels, shards(): pl.pallas_call(exchange_kernel, out_shape=jax.ShapeDtypeStruct((count, wi...  57 us
    unnamed x35, local copies, waits for them, and re-layouts  13 us
    pallas_call x1, Pallas kernels, shards(): pl.pallas_call(functools.partial(mixer_kernel, chunk=chunk), out_shape=(j...  5.53 us

profile of v1, /device:TPU:1, one launch (start us, length us, event | category | flops | bytes accessed | tf_op | source)
XLA Modules:
  0.0 78.4 jit_solution(4049745846898891603)
XLA Ops:
  0.6 0.7 broadcast_in_dim.18.refs_1_
  1.3 0.7 broadcast_in_dim.22.gain
  2.0 0.7 broadcast_in_dim.23.blend
  2.7 0.0 copy-start
  2.7 1.9 %copy-done = f32[24,2,128,128]{3,2,1,0:T(8,128)S(1)} copy-done((f32[24,2,128,128]{3,2,1,0:T(8,128)S(1)}, f32[24,2,128,128]{3,2,1,0:T(8,128)}, u32[]{:S(2)}) %copy-start) | copy-done | bytes 3145752
  4.6 0.0 copy-start.3
  4.6 1.2 %copy-done.3 = bf16[2048,256]{1,0:T(8,128)(2,1)S(1)} copy-done((bf16[2048,256]{1,0:T(8,128)(2,1)S(1)}, bf16[2048,256]{1,0:T(8,128)(2,1)}, u32[]{:S(2)}) %copy-start.3) | copy-done | bytes 1048600
  5.8 0.0 copy-start.4
  5.8 1.2 %copy-done.4 = bf16[2048,256]{1,0:T(8,128)(2,1)S(1)} copy-done((bf16[2048,256]{1,0:T(8,128)(2,1)S(1)}, bf16[2048,256]{1,0:T(8,128)(2,1)}, u32[]{:S(2)}) %copy-start.4) | copy-done | bytes 1048600
  7.1 0.0 copy-start.5
  7.1 1.2 %copy-done.5 = bf16[2048,256]{1,0:T(8,128)(2,1)S(1)} copy-done((bf16[2048,256]{1,0:T(8,128)(2,1)S(1)}, bf16[2048,256]{1,0:T(8,128)(2,1)}, u32[]{:S(2)}) %copy-start.5) | copy-done | bytes 1048600
  8.3 0.0 copy-start.6
  8.3 1.2 %copy-done.6 = bf16[2048,256]{1,0:T(8,128)(2,1)S(1)} copy-done((bf16[2048,256]{1,0:T(8,128)(2,1)S(1)}, bf16[2048,256]{1,0:T(8,128)(2,1)}, u32[]{:S(2)}) %copy-start.6) | copy-done | bytes 1048600
  9.5 0.0 copy-start.7
  9.5 1.2 %copy-done.7 = bf16[256,2048]{1,0:T(8,128)(2,1)S(1)} copy-done((bf16[256,2048]{1,0:T(8,128)(2,1)S(1)}, bf16[256,2048]{1,0:T(8,128)(2,1)}, u32[]{:S(2)}) %copy-start.7) | copy-done | bytes 1048600
  10.7 0.0 copy-start.8
  10.7 0.9 %copy-done.8 = bf16[24,2048]{1,0:T(8,128)(2,1)S(1)} copy-done((bf16[24,2048]{1,0:T(8,128)(2,1)S(1)}, bf16[24,2048]{1,0:T(8,128)(2,1)}, u32[]{:S(2)}) %copy-start.8) | copy-done | bytes 98328
  11.6 0.0 copy-start.10
  11.6 0.8 copy-done.10
  12.4 0.0 copy-start.11
  12.4 0.8 copy-done.11
  13.1 0.0 copy-start.14
  13.1 0.7 copy-done.14
  13.8 0.0 copy-start.15
  13.8 0.7 copy-done.15
  14.4 0.0 copy-start.16
  14.4 0.7 copy-done.16
  15.1 0.0 copy-start.1
  15.1 0.0 copy-start.2
  15.1 0.0 copy-start.9
  15.1 0.0 copy-start.12
  15.1 0.0 copy-start.13
  15.1 5.5 %mixer.1 = (bf16[4,24,512]{2,1,0:T(8,128)(2,1)S(1)}, f32[24,2,128,128]{3,2,1,0:T(8,128)}) custom-call(bf16[24,2048]{1,0:T(8,128)(2,1)S(1)} %copy-done.8, bf16[1,2048]{1,0:T(2,128)(2,1)S(1)} %broadcast_in_dim.18.refs_1_, bf16[8,2048]{1,0:T(8,128)(2,1)S(1)} %bitcast.7, bf16[8,2048]{1,0:T(8,128)(2,1)S(1)} %bitcast.8, f32[1,8]{1,0:T(1,128)S(1)} %bitcast.11, ...), custom_call_target="tpu_custom_call" | custom-call | tf_op jit(solution)/shard_map/mixer/pallas_call | solution.py:384
  20.7 0.0 copy-done.1
  20.7 0.0 copy-done.2
  20.7 0.0 copy-done.9
  20.7 0.0 copy-done.12
  20.7 0.0 copy-done.13
  20.7 57.0 %exchange.1 = bf16[24,2048]{1,0:T(8,128)(2,1)S(1)} custom-call(bf16[4,24,512]{2,1,0:T(8,128)(2,1)S(1)} %get-tuple-element.4.mixed, bf16[24,2048]{1,0:T(8,128)(2,1)S(1)} %copy-done.9, bf16[1,2048]{1,0:T(2,128)(2,1)S(1)} %broadcast_in_dim.22.gain, bf16[1,2048]{1,0:T(2,128)(2,1)S(1)} %broadcast_in_dim.23.blend, s32[6,24]{1,0:T(8,128)S(1)} %bitcast.9, ...), custom_call_target="tpu_custom_call" | custom-call | tf_op jit(solution)/shard_map/exchange/pallas_call | solution.py:410
  77.7 0.6 copy.26
Async XLA Ops:
  2.7 1.9 %copy-start = (f32[24,2,128,128]{3,2,1,0:T(8,128)S(1)}, f32[24,2,128,128]{3,2,1,0:T(8,128)}, u32[]{:S(2)}) copy-start(f32[24,2,128,128]{3,2,1,0:T(8,128)} %refs_12_.1) | copy-start | bytes 9437188
  4.6 1.2 %copy-start.3 = (bf16[2048,256]{1,0:T(8,128)(2,1)S(1)}, bf16[2048,256]{1,0:T(8,128)(2,1)}, u32[]{:S(2)}) copy-start(bf16[2048,256]{1,0:T(8,128)(2,1)} %refs_7_.1) | copy-start | bytes 3145732
  5.8 1.2 %copy-start.4 = (bf16[2048,256]{1,0:T(8,128)(2,1)S(1)}, bf16[2048,256]{1,0:T(8,128)(2,1)}, u32[]{:S(2)}) copy-start(bf16[2048,256]{1,0:T(8,128)(2,1)} %refs_8_.1) | copy-start | bytes 3145732
  7.1 1.2 %copy-start.5 = (bf16[2048,256]{1,0:T(8,128)(2,1)S(1)}, bf16[2048,256]{1,0:T(8,128)(2,1)}, u32[]{:S(2)}) copy-start(bf16[2048,256]{1,0:T(8,128)(2,1)} %refs_9_.1) | copy-start | bytes 3145732
  8.3 1.2 %copy-start.6 = (bf16[2048,256]{1,0:T(8,128)(2,1)S(1)}, bf16[2048,256]{1,0:T(8,128)(2,1)}, u32[]{:S(2)}) copy-start(bf16[2048,256]{1,0:T(8,128)(2,1)} %refs_10_.1) | copy-start | bytes 3145732
  9.5 1.2 %copy-start.7 = (bf16[256,2048]{1,0:T(8,128)(2,1)S(1)}, bf16[256,2048]{1,0:T(8,128)(2,1)}, u32[]{:S(2)}) copy-start(bf16[256,2048]{1,0:T(8,128)(2,1)} %refs_11_.1) | copy-start | bytes 3145732
  10.7 0.9 %copy-start.8 = (bf16[24,2048]{1,0:T(8,128)(2,1)S(1)}, bf16[24,2048]{1,0:T(8,128)(2,1)}, u32[]{:S(2)}) copy-start(bf16[24,2048]{1,0:T(8,128)(2,1)} %tokens.1) | copy-start | bytes 294916
  11.6 0.8 copy-start.10
  12.4 0.8 copy-start.11
  13.1 0.7 copy-start.14
  13.8 0.7 copy-start.15
  14.4 0.7 copy-start.16
  15.1 5.6 %copy-start.1 = (bf16[2048,512]{1,0:T(8,128)(2,1)S(1)}, bf16[2048,512]{1,0:T(8,128)(2,1)}, u32[]{:S(2)}) copy-start(bf16[2048,512]{1,0:T(8,128)(2,1)} %dense_gate.1) | copy-start | bytes 6291460
  15.1 5.6 %copy-start.2 = (bf16[2048,512]{1,0:T(8,128)(2,1)S(1)}, bf16[2048,512]{1,0:T(8,128)(2,1)}, u32[]{:S(2)}) copy-start(bf16[2048,512]{1,0:T(8,128)(2,1)} %dense_up.1) | copy-start | bytes 6291460
  15.1 5.6 %copy-start.9 = (bf16[24,2048]{1,0:T(8,128)(2,1)S(1)}, bf16[24,2048]{1,0:T(8,128)(2,1)}, u32[]{:S(2)}) copy-start(bf16[24,2048]{1,0:T(8,128)(2,1)} %tokens.1) | copy-start | bytes 294916
  15.1 5.6 %copy-start.12 = (s32[24,6]{0,1:T(8,128)S(1)}, s32[24,6]{0,1:T(8,128)}, u32[]{:S(2)}) copy-start(s32[24,6]{0,1:T(8,128)} %param.44) | copy-start | bytes 1732
  15.1 5.6 %copy-start.13 = (f32[24,6]{0,1:T(8,128)S(1)}, f32[24,6]{0,1:T(8,128)}, u32[]{:S(2)}) copy-start(f32[24,6]{0,1:T(8,128)} %param.45) | copy-start | bytes 1732

commit v2 on v1

--- a/solution.py
+++ b/solution.py
@@ -1,5 +1,3 @@
-import functools
-
 import jax
 import jax.numpy as jnp
 from jax import lax
@@ -40,33 +38,29 @@
     return jnp.transpose(jnp.concatenate([x, jnp.zeros((width - rows, width), F32)], axis=0))
 
 
+def row_of(table):
+    return jnp.concatenate([table[i : i + 1, :] for i in range(table.shape[0])], axis=1)
+
+
+def fetch(pairs, sem):
+    copies = [pltpu.make_async_copy(src, dst, sem.at[i]) for i, (src, dst) in enumerate(pairs)]
+    for copy in copies:
+        copy.start()
+    return copies
+
+
 def mixer(
     tokens, first_gain, beta_t, decay_t, rate, bias, head_gain,
-    query_w, key_w, value_w, gate_w, out_w, state,
-    mixed, new_state,
-    weights, out_weights, held, read, in_sem, state_sem, back_sem,
-    chunk,
+    mixed, new_state, weights, out_weights, held, read, loads, pieces, back_sem,
 ):
     rows, width = tokens.shape
     heads, size = held.shape[1], held.shape[2]
-    chunks = rows // chunk
-    loads = [
-        pltpu.make_async_copy(w, weights.at[i], in_sem.at[i])
-        for i, w in enumerate((key_w, value_w, query_w, gate_w))
-    ]
-    loads.append(pltpu.make_async_copy(out_w, out_weights, in_sem.at[4]))
-    pieces = [
-        pltpu.make_async_copy(
-            state.at[pl.ds(c * chunk, chunk)], held.at[pl.ds(c * chunk, chunk)], state_sem.at[c]
-        )
-        for c in range(chunks)
-    ]
-    for copy in loads[:4] + pieces + loads[4:]:
-        copy.start()
-
+    chunks = len(pieces)
+    chunk = rows // chunks
     x = tokens[...].astype(F32)
     total = jnp.sum(x * x, axis=-1, keepdims=True)
-    normed = (x * rms_inverse(total, width) * first_gain[...].astype(F32)).astype(BF16)
+    first = row_of(first_gain[...].astype(F32))
+    normed = (x * rms_inverse(total, width) * first).astype(BF16)
 
     def across(w):
         return lax.dot_general(normed, w[...], (((1,), (1,)), ((), ())), preferred_element_type=F32)
@@ -133,24 +127,23 @@
     return backs
 
 
-def mixer_kernel(*refs, chunk):
-    for back in mixer(*refs, chunk=chunk):
-        back.wait()
-
-
 def spread(table, fill):
     k, tokens = table.shape
     side = jnp.full((k, PAD - tokens), fill, table.dtype)
     return jnp.concatenate([table, side] * Q, axis=1)
 
 
-def exchange_kernel(
-    mixed, tokens, gain, blend, ids, scales,
+def layer_kernel(
+    tokens_h, first_gain_h, beta_h, decay_h, rate_h, bias_h, head_gain_h, gain_h, blend_h, ids_h, scales_h,
+    query_w, key_w, value_w, gate_w, out_w, state,
     dense_gate, dense_up, dense_down, expert_gate, expert_up, expert_down,
-    new_tokens,
+    new_tokens, new_state,
+    tokens, first_gain, beta_t, decay_t, rate, bias, head_gain, gain, blend, ids, scales,
+    weights, out_weights, held, read,
     w_gate, w_up, w_down, e_gate, e_up, e_down,
-    pair_in, chip_sum, chip_in, pair_in2, part2, chip_sum2, chip_in2,
+    mixed, pair_in, chip_sum, chip_in, part2, pair_in2, chip_sum2, chip_in2,
     rows_mid, full_mid, out_box, in_box, wide, back_box, got_box, combined,
+    small_sem, in_sem, state_sem, back_sem,
     w_sem, pair_sem, chip_send, chip_recv, go_send, go_recv, back_send, back_recv,
 ):
     groups = lax.axis_size("ep")
@@ -165,21 +158,46 @@
     def place(i):
         return lax.rem(ep + i, groups), lax.rem(tp + 2 * lax.rem(i, 2), 4)
 
-    loads = [
-        pltpu.make_async_copy(src, dst, w_sem.at[n])
-        for n, (src, dst) in enumerate(
-            (
-                (dense_gate, w_gate),
-                (dense_up, w_up),
-                (dense_down, w_down),
-                (expert_gate.at[0], e_gate),
-                (expert_up.at[0], e_up),
-                (expert_down.at[0], e_down),
-            )
-        )
-    ]
-    for load in loads:
-        load.start()
+    small = fetch(
+        (
+            (ids_h, ids),
+            (scales_h, scales),
+            (tokens_h, tokens),
+            (first_gain_h, first_gain),
+            (beta_h, beta_t),
+            (decay_h, decay_t),
+            (rate_h, rate),
+            (bias_h, bias),
+            (head_gain_h, head_gain),
+            (gain_h, gain),
+            (blend_h, blend),
+        ),
+        small_sem,
+    )
+    chunk = 4
+    mix_loads = fetch(
+        [(w, weights.at[i]) for i, w in enumerate((key_w, value_w, query_w, gate_w))], in_sem
+    )
+    pieces = fetch(
+        [
+            (state.at[pl.ds(c, chunk)], held.at[pl.ds(c, chunk)])
+            for c in range(0, count, chunk)
+        ],
+        state_sem,
+    )
+    out_load = pltpu.make_async_copy(out_w, out_weights, in_sem.at[4])
+    out_load.start()
+    loads = fetch(
+        (
+            (dense_gate, w_gate),
+            (dense_up, w_up),
+            (dense_down, w_down),
+            (expert_gate.at[0], e_gate),
+            (expert_up.at[0], e_up),
+            (expert_down.at[0], e_down),
+        ),
+        w_sem,
+    )
 
     barrier = pltpu.get_barrier_semaphore()
 
@@ -192,8 +210,6 @@
         pl.semaphore_signal(
             barrier, inc=1, device_id=(ep, lax.rem(tp + i, 4)), device_id_type=MESH
         )
-    pl.semaphore_wait(barrier, groups - 1 + 3)
-
     def over_tp(part, pair_buffer, total, chip_buffer, n, between):
         pair = pltpu.make_async_remote_copy(
             src_ref=part, dst_ref=pair_buffer, send_sem=pair_sem.at[2 * n], recv_sem=pair_sem.at[2 * n + 1],
@@ -255,10 +271,24 @@
         tables["pick"] = jnp.where(taken, 1.0, 0.0).astype(BF16)
         tables["weight"] = jnp.transpose(jnp.where(taken, weight, 0.0))
 
-    sends = over_tp(mixed, pair_in, chip_sum, chip_in, 0, build_tables)
-    rows_mid[...] = jnp.zeros_like(rows_mid)
-    finish(sends, chip_sum, chip_in, 0)
-
+    for copy in small:
+        copy.wait()
+    with jax.named_scope("tables"):
+        build_tables()
+        rows_mid[...] = jnp.zeros_like(rows_mid)
+    with jax.named_scope("mixer"):
+        backs = mixer(
+            tokens, first_gain, beta_t, decay_t, rate, bias, head_gain,
+            mixed, new_state, weights, out_weights, held, read, mix_loads + [out_load], pieces, back_sem,
+        )
+    with jax.named_scope("barrier"):
+        pl.semaphore_wait(barrier, groups - 1 + 3)
+    with jax.named_scope("tp_sum"):
+        sends = over_tp(mixed, pair_in, chip_sum, chip_in, 0, lambda: None)
+        finish(sends, chip_sum, chip_in, 0)
+
+    gains = row_of(gain[...].astype(F32))
+    blends = row_of(blend[...].astype(F32))
     residual = []
     squares = jnp.zeros((count, 1), F32)
     for q in range(Q):
@@ -271,11 +301,11 @@
     blended = jnp.zeros((count, 1), F32)
     for q in range(Q):
         part = slice(q * columns, (q + 1) * columns)
-        mid = (residual[q] * inverse * gain[:, part].astype(F32)).astype(BF16)
+        mid = (residual[q] * inverse * gains[:, part]).astype(BF16)
         rows_mid[q * PAD : q * PAD + count, :] = mid
         full_mid[:, part] = mid
         blended += jnp.sum(
-            mid.astype(F32) * blend[:, part].astype(F32), axis=-1, keepdims=True
+            mid.astype(F32) * blends[:, part], axis=-1, keepdims=True
         )
     blend_gate = jax.nn.sigmoid(blended)
     outgoing = dot(tables["pick"], rows_mid[...]).astype(BF16)
@@ -309,7 +339,8 @@
         src_ref=out_box.at[rest], dst_ref=in_box.at[rest], send_sem=go_send, recv_sem=go_recv,
         device_id=(ep, partner), device_id_type=MESH,
     )
-    arrived.wait_recv()
+    with jax.named_scope("go_wait"):
+        arrived.wait_recv()
     tiles = columns // 128
     flat = in_box[...].reshape(slots, columns).astype(F32)
     for t in range(tiles):
@@ -351,19 +382,23 @@
         src_ref=back_box.at[rest], dst_ref=got_box.at[rest], send_sem=back_send, recv_sem=back_recv,
         device_id=(ep, partner), device_id_type=MESH,
     )
-    returned.wait_recv()
+    with jax.named_scope("back_wait"):
+        returned.wait_recv()
     results = got_box[...].reshape(slots, columns)
     routed = dot(high, results) + dot(low, results)
     for q in range(Q):
         part2[q] = (combined[q] + routed[q * PAD : q * PAD + count, :]).astype(BF16)
 
-    sends = over_tp(part2, pair_in2, chip_sum2, chip_in2, 1, lambda: None)
-    finish(sends, chip_sum2, chip_in2, 1)
+    with jax.named_scope("tp_sum2"):
+        sends = over_tp(part2, pair_in2, chip_sum2, chip_in2, 1, lambda: None)
+        finish(sends, chip_sum2, chip_in2, 1)
     for q in range(Q):
         part = slice(q * columns, (q + 1) * columns)
         more = chip_sum2[q].astype(F32) + chip_in2[q].astype(F32)
         new_tokens[:, part] = (residual[q] + more).astype(BF16)
     returned.wait_send()
+    for back in backs:
+        back.wait()
 
 
 def shards(
@@ -380,46 +415,39 @@
     expert_hidden = expert_gate.shape[2]
     anywhere = pl.BlockSpec(memory_space=pl.ANY)
     near = pl.BlockSpec(memory_space=VMEM)
-    chunk = 4
-    mixed, new_state = pl.pallas_call(
-        functools.partial(mixer_kernel, chunk=chunk),
+    wire = VMEM((Q, count, columns), BF16)
+    box = VMEM((groups, CAP * Q, columns), BF16)
+    new_tokens, new_state = pl.pallas_call(
+        layer_kernel,
         out_shape=(
-            jax.ShapeDtypeStruct((Q, count, columns), BF16),
+            jax.ShapeDtypeStruct((count, width), BF16),
             jax.ShapeDtypeStruct(delta_state.shape, F32),
         ),
-        in_specs=[near] * 7 + [anywhere] * 6,
+        in_specs=[anywhere] * 23,
         out_specs=(near, anywhere),
         scratch_shapes=[
+            VMEM((count, width), BF16),
+            VMEM((width // 128, 128), BF16),
+            VMEM((8, width), BF16),
+            VMEM((8, width), BF16),
+            VMEM((1, 8), F32),
+            VMEM((1, 8), F32),
+            VMEM((1, size), BF16),
+            VMEM((width // 128, 128), BF16),
+            VMEM((width // 128, 128), BF16),
+            VMEM(route_ids.shape[::-1], jnp.int32),
+            VMEM(route_ids.shape[::-1], F32),
             VMEM((4, width, heads * size), BF16),
             VMEM((heads * size, width), BF16),
             VMEM(delta_state.shape, F32),
             VMEM((count, heads * size), F32),
-            pltpu.SemaphoreType.DMA((5,)),
-            pltpu.SemaphoreType.DMA((count // chunk,)),
-            pltpu.SemaphoreType.DMA((count // chunk,)),
-        ],
-        compiler_params=pltpu.CompilerParams(vmem_limit_bytes=32 << 20),
-        name="mixer",
-    )(
-        tokens, first_gain[None], beta_weight.T, decay_weight.T, decay_rate[None],
-        decay_bias[None], head_gain[None],
-        query_weight, key_weight, value_weight, outgate_weight, out_weight, delta_state,
-    )
-    wire = VMEM((Q, count, columns), BF16)
-    box = VMEM((groups, CAP * Q, columns), BF16)
-    new_tokens = pl.pallas_call(
-        exchange_kernel,
-        out_shape=jax.ShapeDtypeStruct((count, width), BF16),
-        in_specs=[near] * 6 + [anywhere] * 6,
-        out_specs=near,
-        scratch_shapes=[
             VMEM((width, hidden), BF16),
             VMEM((width, hidden), BF16),
             VMEM((hidden, width), BF16),
             VMEM((width, expert_hidden), BF16),
             VMEM((width, expert_hidden), BF16),
             VMEM((expert_hidden, width), BF16),
-            wire, wire, wire, wire, wire, wire, wire,
+            wire, wire, wire, wire, wire, wire, wire, wire,
             VMEM((Q * PAD, columns), BF16),
             VMEM((count, width), BF16),
             box,
@@ -428,6 +456,10 @@
             box,
             box,
             VMEM((Q, count, columns), F32),
+            pltpu.SemaphoreType.DMA((11,)),
+            pltpu.SemaphoreType.DMA((5,)),
+            pltpu.SemaphoreType.DMA((6,)),
+            pltpu.SemaphoreType.DMA((6,)),
             pltpu.SemaphoreType.DMA((6,)),
             pltpu.SemaphoreType.DMA((4,)),
             pltpu.SemaphoreType.DMA((2, 2)),
@@ -438,11 +470,14 @@
             pltpu.SemaphoreType.DMA,
         ],
         compiler_params=pltpu.CompilerParams(
-            collective_id=0, has_side_effects=True, vmem_limit_bytes=48 << 20
+            collective_id=0, has_side_effects=True, vmem_limit_bytes=67043328
         ),
-        name="exchange",
+        name="layer",
     )(
-        mixed, tokens, second_gain[None], blend_weight[None], route_ids.T, route_weights.T,
+        tokens, first_gain.reshape(-1, 128), beta_weight.T, decay_weight.T, decay_rate[None],
+        decay_bias[None], head_gain[None], second_gain.reshape(-1, 128), blend_weight.reshape(-1, 128),
+        route_ids.T, route_weights.T,
+        query_weight, key_weight, value_weight, outgate_weight, out_weight, delta_state,
         dense_gate_weight, dense_up_weight, dense_down_weight,
         expert_gate, expert_up, expert_down,
     )

time: 79 us -> 67 us (0.85)
  local copies, waits for them, and re-layouts: 15.1 us -> 5.45 us
  Pallas kernels: 62.5 us -> 60.3 us
    unnamed x35 -> x2, local copies, waits for them, and re-layouts: 13 us -> 5.45 us
    pallas_call x2 -> x1, Pallas kernels: 62.5 us -> 60.3 us  [shards(): pl.pallas_call(layer_kernel, out_shape=(jax.ShapeDtypeStruct((count, widt...]
    broadcast_in_dim x3 -> x0, local copies, waits for them, and re-layouts: 2.08 us -> none  [the longest x1 0.69 us: shards(): first_gain[None]]
where the time goes in v2:
time: 67 us; the launch traced here: 66.4 us
  Pallas kernels  60.3 us (90%)
  local copies, waits for them, and re-layouts  5.45 us (8%)
    pallas_call x1, Pallas kernels, shards(): pl.pallas_call(layer_kernel, out_shape=(jax.ShapeDtypeStruct((count, widt...  60.3 us
    unnamed x2, local copies, waits for them, and re-layouts  5.45 us

profile of v2, /device:TPU:1, one launch (start us, length us, event | category | flops | bytes accessed | tf_op | source)
XLA Modules:
  0.0 66.4 jit_solution(2758192802472139319)
XLA Ops:
  0.6 60.3 %layer.1 = (bf16[24,2048]{1,0:T(8,128)(2,1)}, f32[24,2,128,128]{3,2,1,0:T(8,128)}) custom-call(bf16[24,2048]{1,0:T(8,128)(2,1)} %tokens_h.1, bf16[16,128]{1,0:T(8,128)(2,1)} %bitcast.12, bf16[8,2048]{1,0:T(8,128)(2,1)} %bitcast.10, bf16[8,2048]{1,0:T(8,128)(2,1)} %bitcast.11, f32[1,8]{1,0:T(1,128)} %bitcast.17, f32[1,8]{1,0:T(1,128)} %bitcast.18, ...), custom_call_target="tpu_custom_call" | custom-call | tf_op jit(solution)/shard_map/layer/pallas_call | solution.py:420
  60.9 1.5 %copy.27 = bf16[24,2048]{1,0:T(8,128)(2,1)} copy(bf16[24,2048]{1,0:T(8,128)(2,1)} %get-tuple-element.4) | data formatting | bytes 196608
  62.5 3.9 %copy.28 = f32[24,2,128,128]{3,2,1,0:T(8,128)} copy(f32[24,2,128,128]{3,2,1,0:T(8,128)} %get-tuple-element.5) | data formatting | bytes 6291456

commit v3 on v2

--- a/solution.py
+++ b/solution.py
@@ -15,6 +15,7 @@
 Q = 4
 PAD = 32
 CAP = 2
+PARTS = 4
 
 
 def silu(x):
@@ -51,7 +52,7 @@
 
 def mixer(
     tokens, first_gain, beta_t, decay_t, rate, bias, head_gain,
-    mixed, new_state, weights, out_weights, held, read, loads, pieces, back_sem,
+    mixed, new_state, weights, out_weights, held, read, loads, pieces, back_sem, then,
 ):
     rows, width = tokens.shape
     heads, size = held.shape[1], held.shape[2]
@@ -83,6 +84,7 @@
         return dot(normed, weights[i]).astype(BF16).astype(F32)
 
     key_raw, value_raw, query_raw, gate_raw = [project(i) for i in range(4)]
+    then()
     keys, queries, values, betas, decays = [], [], [], [], []
     for h in range(heads):
         part = slice(h * size, (h + 1) * size)
@@ -187,18 +189,6 @@
     )
     out_load = pltpu.make_async_copy(out_w, out_weights, in_sem.at[4])
     out_load.start()
-    loads = fetch(
-        (
-            (dense_gate, w_gate),
-            (dense_up, w_up),
-            (dense_down, w_down),
-            (expert_gate.at[0], e_gate),
-            (expert_up.at[0], e_up),
-            (expert_down.at[0], e_down),
-        ),
-        w_sem,
-    )
-
     barrier = pltpu.get_barrier_semaphore()
 
     def greet(i, carry):
@@ -244,6 +234,7 @@
             send.wait_send()
 
     slots = groups * CAP * Q
+    each = groups // PARTS
     lanes = Q * PAD
     tables = {}
 
@@ -252,7 +243,7 @@
         raw = scales[...]
         scale_c = spread(raw / jnp.sum(raw, axis=0, keepdims=True) * ROUTED_SCALE, 0.0)
         row = lax.broadcasted_iota(jnp.int32, (slots, 1), 0)
-        offset = row // (CAP * Q)
+        offset = lax.rem(row // (CAP * Q), each) * PARTS + row // (CAP * Q * each)
         expert = lax.rem(ep + offset, groups) * 4 + lax.rem(tp + 2 * lax.rem(offset, 2), 4)
         named = jnp.zeros((slots, lanes), F32)
         weight = jnp.zeros((slots, lanes), F32)
@@ -271,15 +262,36 @@
         tables["pick"] = jnp.where(taken, 1.0, 0.0).astype(BF16)
         tables["weight"] = jnp.transpose(jnp.where(taken, weight, 0.0))
 
-    for copy in small:
+    loads = []
+
+    def fetch_rest():
+        loads.extend(
+            fetch(
+                (
+                    (dense_gate, w_gate),
+                    (dense_up, w_up),
+                    (dense_down, w_down),
+                    (expert_gate.at[0], e_gate),
+                    (expert_up.at[0], e_up),
+                    (expert_down.at[0], e_down),
+                ),
+                w_sem,
+            )
+        )
+
+    for copy in small[:2]:
         copy.wait()
     with jax.named_scope("tables"):
         build_tables()
         rows_mid[...] = jnp.zeros_like(rows_mid)
+    with jax.named_scope("small"):
+        for copy in small[2:]:
+            copy.wait()
     with jax.named_scope("mixer"):
         backs = mixer(
             tokens, first_gain, beta_t, decay_t, rate, bias, head_gain,
             mixed, new_state, weights, out_weights, held, read, mix_loads + [out_load], pieces, back_sem,
+            fetch_rest,
         )
     with jax.named_scope("barrier"):
         pl.semaphore_wait(barrier, groups - 1 + 3)
@@ -311,17 +323,30 @@
     outgoing = dot(tables["pick"], rows_mid[...]).astype(BF16)
     out_box[...] = outgoing.reshape(out_box.shape)
 
-    def go(i):
+    def send_part(source, target, send_sem, recv_sem, part, sign):
+        def one(j, carry):
+            offset = j * PARTS + part
+            block = part * each + j
+            pltpu.make_async_remote_copy(
+                src_ref=source.at[block], dst_ref=target.at[block],
+                send_sem=send_sem.at[part], recv_sem=recv_sem.at[part],
+                device_id=place(groups + sign * offset), device_id_type=MESH,
+            ).start()
+            return carry
+
+        lax.fori_loop(1 if part == 0 else 0, each, one, 0)
+
+    def whole_part(source, target, send_sem, recv_sem, part):
+        first = 1 if part == 0 else 0
+        blocks = pl.ds(part * each + first, each - first)
         return pltpu.make_async_remote_copy(
-            src_ref=out_box.at[i], dst_ref=in_box.at[i], send_sem=go_send, recv_sem=go_recv,
-            device_id=place(i), device_id_type=MESH,
-        )
-
-    def go_start(i, carry):
-        go(i).start()
-        return carry
-
-    lax.fori_loop(1, groups, go_start, 0)
+            src_ref=source.at[blocks], dst_ref=target.at[blocks],
+            send_sem=send_sem.at[part], recv_sem=recv_sem.at[part],
+            device_id=(ep, partner), device_id_type=MESH,
+        )
+
+    for part in range(PARTS):
+        send_part(out_box, in_box, go_send, go_recv, part, 1)
     in_box[0] = out_box[0]
 
     for n in range(3):
@@ -334,58 +359,48 @@
     for n in range(3, 6):
         loads[n].wait()
 
-    rest = pl.ds(1, groups - 1)
-    arrived = pltpu.make_async_remote_copy(
-        src_ref=out_box.at[rest], dst_ref=in_box.at[rest], send_sem=go_send, recv_sem=go_recv,
-        device_id=(ep, partner), device_id_type=MESH,
-    )
-    with jax.named_scope("go_wait"):
-        arrived.wait_recv()
     tiles = columns // 128
-    flat = in_box[...].reshape(slots, columns).astype(F32)
-    for t in range(tiles):
-        wide[t] = flat[:, t * 128 : (t + 1) * 128]
-    count_slots = groups * CAP
-    gate_part = jnp.zeros((count_slots, hidden_size), F32)
-    up_part = jnp.zeros((count_slots, hidden_size), F32)
-    for q in range(Q):
-        part = slice(q * columns, (q + 1) * columns)
-        block = jnp.concatenate(
-            [wide[t, pl.ds(q, count_slots, stride=Q), :] for t in range(tiles)], axis=1
+    rows = each * CAP
+    for part in range(PARTS):
+        with jax.named_scope("go_wait"):
+            whole_part(out_box, in_box, go_send, go_recv, part).wait_recv()
+        blocks = pl.ds(part * each, each)
+        base = part * rows * Q
+        flat = in_box[blocks].reshape(rows * Q, columns).astype(F32)
+        for t in range(tiles):
+            wide[t, base : base + rows * Q] = flat[:, t * 128 : (t + 1) * 128]
+        gate_part = jnp.zeros((rows, hidden_size), F32)
+        up_part = jnp.zeros((rows, hidden_size), F32)
+        for q in range(Q):
+            columns_q = slice(q * columns, (q + 1) * columns)
+            block = jnp.concatenate(
+                [wide[t, pl.ds(base + q, rows, stride=Q), :] for t in range(tiles)], axis=1
+            ).astype(BF16)
+            gate_part += dot(block, e_gate[columns_q, :])
+            up_part += dot(block, e_up[columns_q, :])
+        hidden = (silu(gate_part) * up_part).astype(BF16)
+        for q in range(Q):
+            down = dot(hidden, e_down[:, q * columns : (q + 1) * columns])
+            for t in range(tiles):
+                wide[t, pl.ds(base + q, rows, stride=Q), :] = down[:, t * 128 : (t + 1) * 128]
+        back = jnp.concatenate(
+            [wide[t, base : base + rows * Q] for t in range(tiles)], axis=1
         ).astype(BF16)
-        gate_part += dot(block, e_gate[part, :])
-        up_part += dot(block, e_up[part, :])
-    hidden = (silu(gate_part) * up_part).astype(BF16)
-    for q in range(Q):
-        part = slice(q * columns, (q + 1) * columns)
-        down = dot(hidden, e_down[:, part])
-        for t in range(tiles):
-            wide[t, pl.ds(q, count_slots, stride=Q), :] = down[:, t * 128 : (t + 1) * 128]
-    back = jnp.concatenate([wide[t] for t in range(tiles)], axis=1).astype(BF16)
-    back_box[...] = back.reshape(back_box.shape)
-
-    def back_start(i, carry):
-        group, lane = place(groups - i)
-        pltpu.make_async_remote_copy(
-            src_ref=back_box.at[i], dst_ref=got_box.at[i], send_sem=back_send, recv_sem=back_recv,
-            device_id=(group, lane), device_id_type=MESH,
-        ).start()
-        return carry
-
-    lax.fori_loop(1, groups, back_start, 0)
+        back_box[blocks] = back.reshape(each, CAP * Q, columns)
+        send_part(back_box, got_box, back_send, back_recv, part, -1)
     got_box[0] = back_box[0]
     weight = tables["weight"]
     high = weight.astype(BF16)
     low = (weight - high.astype(F32)).astype(BF16)
-    arrived.wait_send()
-    returned = pltpu.make_async_remote_copy(
-        src_ref=back_box.at[rest], dst_ref=got_box.at[rest], send_sem=back_send, recv_sem=back_recv,
-        device_id=(ep, partner), device_id_type=MESH,
-    )
-    with jax.named_scope("back_wait"):
-        returned.wait_recv()
-    results = got_box[...].reshape(slots, columns)
-    routed = dot(high, results) + dot(low, results)
+    for part in range(PARTS):
+        whole_part(out_box, in_box, go_send, go_recv, part).wait_send()
+    routed = jnp.zeros((lanes, columns), F32)
+    for part in range(PARTS):
+        with jax.named_scope("back_wait"):
+            whole_part(back_box, got_box, back_send, back_recv, part).wait_recv()
+        results = got_box[pl.ds(part * each, each)].reshape(rows * Q, columns)
+        some = slice(part * rows * Q, (part + 1) * rows * Q)
+        routed += dot(high[:, some], results) + dot(low[:, some], results)
     for q in range(Q):
         part2[q] = (combined[q] + routed[q * PAD : q * PAD + count, :]).astype(BF16)
 
@@ -396,7 +411,8 @@
         part = slice(q * columns, (q + 1) * columns)
         more = chip_sum2[q].astype(F32) + chip_in2[q].astype(F32)
         new_tokens[:, part] = (residual[q] + more).astype(BF16)
-    returned.wait_send()
+    for part in range(PARTS):
+        whole_part(back_box, got_box, back_send, back_recv, part).wait_send()
     for back in backs:
         back.wait()
 
@@ -464,10 +480,10 @@
             pltpu.SemaphoreType.DMA((4,)),
             pltpu.SemaphoreType.DMA((2, 2)),
             pltpu.SemaphoreType.DMA((2, 2)),
-            pltpu.SemaphoreType.DMA,
-            pltpu.SemaphoreType.DMA,
-            pltpu.SemaphoreType.DMA,
-            pltpu.SemaphoreType.DMA,
+            pltpu.SemaphoreType.DMA((PARTS,)),
+            pltpu.SemaphoreType.DMA((PARTS,)),
+            pltpu.SemaphoreType.DMA((PARTS,)),
+            pltpu.SemaphoreType.DMA((PARTS,)),
         ],
         compiler_params=pltpu.CompilerParams(
             collective_id=0, has_side_effects=True, vmem_limit_bytes=67043328

time: 67 us -> 60.4 us (0.901)
  Pallas kernels: 60.3 us -> 54.1 us
    pallas_call x1, Pallas kernels: 60.3 us -> 54.1 us  [shards(): pl.pallas_call(layer_kernel, out_shape=(jax.ShapeDtypeStruct((count, widt...]
where the time goes in v3:
time: 60.4 us; the launch traced here: 60.2 us
  Pallas kernels  54.1 us (90%)
  local copies, waits for them, and re-layouts  5.45 us (9%)
  between operations  0.65 us (1%)
    pallas_call x1, Pallas kernels, shards(): pl.pallas_call(layer_kernel, out_shape=(jax.ShapeDtypeStruct((count, widt...  54.1 us
    unnamed x2, local copies, waits for them, and re-layouts  5.45 us

profile of v3, /device:TPU:1, one launch (start us, length us, event | category | flops | bytes accessed | tf_op | source)
XLA Modules:
  0.0 60.2 jit_solution(9085367188696940996)
XLA Ops:
  0.6 54.1 %layer.1 = (bf16[24,2048]{1,0:T(8,128)(2,1)}, f32[24,2,128,128]{3,2,1,0:T(8,128)}) custom-call(bf16[24,2048]{1,0:T(8,128)(2,1)} %tokens_h.1, bf16[16,128]{1,0:T(8,128)(2,1)} %bitcast.12, bf16[8,2048]{1,0:T(8,128)(2,1)} %bitcast.10, bf16[8,2048]{1,0:T(8,128)(2,1)} %bitcast.11, f32[1,8]{1,0:T(1,128)} %bitcast.17, f32[1,8]{1,0:T(1,128)} %bitcast.18, ...), custom_call_target="tpu_custom_call" | custom-call | tf_op jit(solution)/shard_map/layer/pallas_call | solution.py:436
  54.8 1.5 %copy.27 = bf16[24,2048]{1,0:T(8,128)(2,1)} copy(bf16[24,2048]{1,0:T(8,128)(2,1)} %get-tuple-element.4) | data formatting | bytes 196608
  56.3 3.9 %copy.28 = f32[24,2,128,128]{3,2,1,0:T(8,128)} copy(f32[24,2,128,128]{3,2,1,0:T(8,128)} %get-tuple-element.5) | data formatting | bytes 6291456

commit v4 on v3

v4 whole, which is shorter than its diff:
```python
import jax
import jax.numpy as jnp
from jax import lax
from jax.experimental import pallas as pl
from jax.experimental.pallas import tpu as pltpu
from jax.sharding import PartitionSpec as P

NORM_EPS = 1e-06
UNIT_EPS = 1e-06
ROUTED_SCALE = 2.5
MESH = pl.DeviceIdType.MESH
F32 = jnp.float32
BF16 = jnp.bfloat16
VMEM = pltpu.VMEM
Q = 4
LANES = 128
PAD = 32
CAP = 2
PARTS = 4


def silu(x):
    return x * jax.nn.sigmoid(x)


def dot(a, b):
    return jnp.dot(a, b, preferred_element_type=F32)


def unit_rows(x):
    return x * lax.rsqrt(jnp.sum(x * x, axis=-1, keepdims=True) + UNIT_EPS)


def rms_inverse(total, width):
    return lax.rsqrt(total * (1.0 / width) + NORM_EPS)


def turned(x):
    rows, width = x.shape
    return jnp.transpose(jnp.concatenate([x, jnp.zeros((width - rows, width), F32)], axis=0))


def row_of(table):
    return jnp.concatenate([table[i : i + 1, :] for i in range(table.shape[0])], axis=1)


def fetch(pairs, sem):
    copies = [pltpu.make_async_copy(src, dst, sem.at[i]) for i, (src, dst) in enumerate(pairs)]
    for copy in copies:
        copy.start()
    return copies


def mixer(
    tokens, first_gain, beta_t, decay_t, rate, bias, head_gain,
    mixed, new_state, weights, out_weights, held, read, loads, pieces, back_sem, then,
):
    rows, width = tokens.shape
    heads, size = held.shape[1], held.shape[2]
    chunks = len(pieces)
    chunk = rows // chunks
    x = tokens[...].astype(F32)
    total = jnp.sum(x * x, axis=-1, keepdims=True)
    first = row_of(first_gain[...].astype(F32))
    normed = (x * rms_inverse(total, width) * first).astype(BF16)

    def across(w):
        return lax.dot_general(normed, w[...], (((1,), (1,)), ((), ())), preferred_element_type=F32)

    beta_all = jax.nn.sigmoid(across(beta_t))
    decay_in = across(decay_t) + bias[...]
    softplus = jnp.maximum(decay_in, 0.0) + jnp.log1p(jnp.exp(-jnp.abs(decay_in)))
    decay_all = jnp.exp(-rate[...] * softplus)
    head_at = lax.broadcasted_iota(jnp.int32, beta_all.shape, 1)
    first_head = lax.axis_index("tp") * heads

    def of_head(values, h):
        column = jnp.sum(
            jnp.where(head_at == first_head + h, values, 0.0), axis=1, keepdims=True
        )
        return jnp.broadcast_to(column, (rows, size))

    def project(i):
        loads[i].wait()
        return dot(normed, weights[i]).astype(BF16).astype(F32)

    key_raw, value_raw, query_raw, gate_raw = [project(i) for i in range(4)]
    then()
    keys, queries, values, betas, decays = [], [], [], [], []
    for h in range(heads):
        part = slice(h * size, (h + 1) * size)
        keys.append(turned(unit_rows(silu(key_raw[:, part]))))
        queries.append(turned(unit_rows(silu(query_raw[:, part])) * size ** (-0.5)))
        values.append(silu(value_raw[:, part]))
        betas.append(of_head(beta_all, h))
        decays.append(of_head(decay_all, h))
    backs = []
    for c in range(chunks):
        pieces[c].wait()
        for s in range(c * chunk, (c + 1) * chunk):
            for h in range(heads):
                key = jnp.broadcast_to(keys[h][:, s : s + 1], (size, size))
                query = jnp.broadcast_to(queries[h][:, s : s + 1], (size, size))
                decayed = held[s, h] * decays[h][s : s + 1, :]
                predicted = jnp.sum(decayed * key, axis=0, keepdims=True)
                change = betas[h][s : s + 1, :] * (values[h][s : s + 1, :] - predicted)
                new = decayed + key * change
                held[s, h] = new
                read[s : s + 1, h * size : (h + 1) * size] = jnp.sum(
                    new * query, axis=0, keepdims=True
                )
        back = pltpu.make_async_copy(
            held.at[pl.ds(c * chunk, chunk)], new_state.at[pl.ds(c * chunk, chunk)], back_sem.at[c]
        )
        back.start()
        backs.append(back)
    gated = []
    for h in range(heads):
        part = slice(h * size, (h + 1) * size)
        r = read[:, part]
        inverse = rms_inverse(jnp.sum(r * r, axis=-1, keepdims=True), size)
        gated.append(
            (r * inverse * head_gain[...].astype(F32) * silu(gate_raw[:, part])).astype(BF16)
        )
    gated = jnp.concatenate(gated, axis=1)
    loads[4].wait()
    columns = width // Q
    for q in range(Q):
        mixed[q] = dot(gated, out_weights[:, q * columns : (q + 1) * columns]).astype(BF16)
    return backs


def layer_kernel(
    tokens_h, first_gain_h, beta_h, decay_h, rate_h, bias_h, head_gain_h, gain_h, blend_h, ids_h, scales_h,
    query_w, key_w, value_w, gate_w, out_w, state,
    dense_gate, dense_up, dense_down, expert_gate, expert_up, expert_down,
    new_tokens, new_state,
    tokens, first_gain, beta_t, decay_t, rate, bias, head_gain, gain, blend, ids, scales,
    weights, out_weights, held, read,
    w_gate, w_up, w_down, e_gate, e_up, e_down,
    mixed, mixed_in, pieces_mid, dense_part, dense_in, final,
    rows_mid, full_mid, out_box, in_box, wide_out, wide, wide_got, back_box, got_box, dense_own,
    small_sem, in_sem, state_sem, back_sem, w_sem, near_send, near_recv, go_send, go_recv, back_send, back_recv,
):
    groups = lax.axis_size("ep")
    ep, tp = lax.axis_index("ep"), lax.axis_index("tp")
    count, width = tokens.shape
    columns = width // Q
    tiles = columns // LANES
    hidden_size = w_gate.shape[1]
    each = groups // PARTS

    small = fetch(
        (
            (ids_h, ids),
            (scales_h, scales),
            (tokens_h, tokens),
            (first_gain_h, first_gain),
            (beta_h, beta_t),
            (decay_h, decay_t),
            (rate_h, rate),
            (bias_h, bias),
            (head_gain_h, head_gain),
            (gain_h, gain),
            (blend_h, blend),
        ),
        small_sem,
    )
    chunk = 4
    mix_loads = fetch(
        [(w, weights.at[i]) for i, w in enumerate((key_w, value_w, query_w, gate_w))], in_sem
    )
    pieces = fetch(
        [
            (state.at[pl.ds(c, chunk)], held.at[pl.ds(c, chunk)])
            for c in range(0, count, chunk)
        ],
        state_sem,
    )
    out_load = pltpu.make_async_copy(out_w, out_weights, in_sem.at[4])
    out_load.start()

    barrier = pltpu.get_barrier_semaphore()

    def greet(i, carry):
        pl.semaphore_signal(
            barrier, inc=1, device_id=(lax.rem(ep + i, groups), tp), device_id_type=MESH
        )
        return carry

    lax.fori_loop(1, groups, greet, 0)
    for u in range(1, Q):
        pl.semaphore_signal(
            barrier, inc=1, device_id=(ep, lax.rem(tp + u, Q)), device_id_type=MESH
        )

    def to_peer(n, u, source, target):
        return pltpu.make_async_remote_copy(
            src_ref=source, dst_ref=target,
            send_sem=near_send.at[n, u], recv_sem=near_recv.at[n, u],
            device_id=(ep, lax.rem(tp + u, Q)), device_id_type=MESH,
        )

    slots = groups * Q * CAP
    loads = []

    def fetch_rest():
        loads.extend(
            fetch(
                (
                    (dense_gate, w_gate),
                    (dense_up, w_up),
                    (dense_down, w_down),
                    (expert_gate.at[0], e_gate),
                    (expert_up.at[0], e_up),
                    (expert_down.at[0], e_down),
                ),
                w_sem,
            )
        )

    for copy in small[:2]:
        copy.wait()
    with jax.named_scope("tables"):
        k_count = ids.shape[0]
        side = LANES - count
        ids_c = jnp.concatenate([ids[...], jnp.full((k_count, side), -1, jnp.int32)], axis=1)
        raw = scales[...]
        scale_c = jnp.concatenate(
            [
                raw / jnp.sum(raw, axis=0, keepdims=True) * ROUTED_SCALE,
                jnp.zeros((k_count, side), F32),
            ],
            axis=1,
        )
        row = lax.broadcasted_iota(jnp.int32, (slots, 1), 0)
        block = row // (Q * CAP)
        offset = lax.rem(block, each) * PARTS + block // each
        expert = lax.rem(ep + offset, groups) * Q + lax.rem(row // CAP, Q)
        named = jnp.zeros((slots, LANES), F32)
        weight = jnp.zeros((slots, LANES), F32)
        for k in range(k_count):
            hit = ids_c[k : k + 1, :] == expert
            named = jnp.where(hit, 1.0, named)
            weight = jnp.where(hit, scale_c[k : k + 1, :], weight)
        a = lax.broadcasted_iota(jnp.int32, (LANES, LANES), 0)
        b = lax.broadcasted_iota(jnp.int32, (LANES, LANES), 1)
        rank = dot(named.astype(BF16), (a < b).astype(F32).astype(BF16))
        taken = (named > 0.5) & (rank == lax.rem(row, CAP).astype(F32))
        pick = jnp.where(taken, 1.0, 0.0).astype(BF16)[:, :PAD]
        weight = jnp.transpose(jnp.where(taken, weight, 0.0))[:PAD, :]
        high = weight.astype(BF16)
        low = (weight - high.astype(F32)).astype(BF16)
        rows_mid[...] = jnp.zeros_like(rows_mid)
    with jax.named_scope("small"):
        for copy in small[2:]:
            copy.wait()
    with jax.named_scope("mixer"):
        backs = mixer(
            tokens, first_gain, beta_t, decay_t, rate, bias, head_gain,
            mixed, new_state, weights, out_weights, held, read, mix_loads + [out_load], pieces, back_sem,
            fetch_rest,
        )
    with jax.named_scope("barrier"):
        pl.semaphore_wait(barrier, groups - 1 + Q - 1)

    with jax.named_scope("mix_sum"):
        sums = [to_peer(0, u, mixed.at[lax.rem(tp + u, Q)], mixed_in.at[u]) for u in range(1, Q)]
        for copy in sums:
            copy.start()
        own = pl.ds(pl.multiple_of(tp * columns, columns), columns)
        mix = mixed[tp].astype(F32)
        for u in range(1, Q):
            sums[u - 1].wait_recv()
            mix += mixed_in[u].astype(F32)
        residual = (tokens[:, own].astype(F32) + mix).astype(BF16)
        rows_mid[:count, :] = residual
        pieces_mid[tp] = residual

    def send_part(source, target, send_sem, recv_sem, part, sign):
        def one(place, group, lane):
            pltpu.make_async_remote_copy(
                src_ref=source.at[place * Q + lane], dst_ref=target.at[place * Q + tp],
                send_sem=send_sem.at[part], recv_sem=recv_sem.at[part],
                device_id=(group, lane), device_id_type=MESH,
            ).start()

        def some(j, carry):
            group = lax.rem(ep + groups + sign * (j * PARTS + part), groups)
            for lane in range(Q):
                one(part * each + j, group, lane)
            return carry

        if part == 0:
            for u in range(1, Q):
                one(0, ep, lax.rem(tp + u, Q))
        lax.fori_loop(1 if part == 0 else 0, each, some, 0)

    def whole_part(source, target, send_sem, recv_sem, part):
        first = 1 if part == 0 else 0
        blocks = pl.ds(part * each * Q + first, each * Q - first)
        return pltpu.make_async_remote_copy(
            src_ref=source.at[blocks], dst_ref=target.at[blocks],
            send_sem=send_sem.at[part], recv_sem=recv_sem.at[part],
            device_id=(ep, lax.rem(tp + 1, Q)), device_id_type=MESH,
        )

    rows = each * Q * CAP
    lines = rows * tiles
    x = rows_mid[...]
    with jax.named_scope("go_start"):
        for part in range(PARTS):
            base = part * lines
            outgoing = dot(pick[part * rows : (part + 1) * rows, :], x)
            for t in range(tiles):
                wide_out[pl.ds(base + t, rows, stride=tiles), :] = outgoing[
                    :, t * LANES : (t + 1) * LANES
                ]
            blocks = pl.ds(part * each * Q, each * Q)
            out_box[blocks] = (
                wide_out[base : base + lines, :].astype(BF16).reshape(each * Q, CAP * tiles, LANES)
            )
            send_part(out_box, in_box, go_send, go_recv, part, 1)
            if part == 0:
                spread = [to_peer(1, u, pieces_mid.at[tp], pieces_mid.at[tp]) for u in range(1, Q)]
                for copy in spread:
                    copy.start()
    in_box[tp] = out_box[tp]

    gains = row_of(gain[...].astype(F32))
    with jax.named_scope("dense"):
        for copy in spread:
            copy.wait_recv()
        squares = jnp.zeros((count, 1), F32)
        for q in range(Q):
            res = pieces_mid[q].astype(F32)
            squares += jnp.sum(res * res, axis=-1, keepdims=True)
        inverse = rms_inverse(squares, width)
        blends = row_of(blend[...].astype(F32))
        blended = jnp.zeros((count, 1), F32)
        for q in range(Q):
            part_q = slice(q * columns, (q + 1) * columns)
            mid = (pieces_mid[q].astype(F32) * inverse * gains[:, part_q]).astype(BF16)
            full_mid[:, part_q] = mid
            blended += jnp.sum(mid.astype(F32) * blends[:, part_q], axis=-1, keepdims=True)
        blend_gate = jax.nn.sigmoid(blended)
        for n in range(3):
            loads[n].wait()
        mid = full_mid[...]
        dense_hidden = (silu(dot(mid, w_gate[...])) * dot(mid, w_up[...])).astype(BF16)
        for q in range(Q):
            dense = blend_gate * dot(dense_hidden, w_down[:, q * columns : (q + 1) * columns])
            dense_own[q] = dense
            dense_part[q] = dense.astype(BF16)
        dense_sums = [
            to_peer(2, u, dense_part.at[lax.rem(tp + u, Q)], dense_in.at[u]) for u in range(1, Q)
        ]
        for copy in dense_sums:
            copy.start()
        for n in range(3, 6):
            loads[n].wait()

    apart = Q * CAP * tiles
    for part in range(PARTS):
        with jax.named_scope("go_wait"):
            whole_part(out_box, in_box, go_send, go_recv, part).wait_recv()
        blocks = pl.ds(part * each * Q, each * Q)
        base = part * lines
        wide[base : base + lines, :] = in_box[blocks].reshape(lines, LANES).astype(F32)

        def at(q, s, t):
            return pl.ds(base + (q * CAP + s) * tiles + t, each, stride=apart)

        arrived = [
            jnp.concatenate(
                [
                    jnp.concatenate([wide[at(q, s, t), :] for t in range(tiles)], axis=1)
                    for s in range(CAP)
                ],
                axis=0,
            )
            for q in range(Q)
        ]
        squares = jnp.zeros((each * CAP, 1), F32)
        for q in range(Q):
            squares += jnp.sum(arrived[q] * arrived[q], axis=-1, keepdims=True)
        inverse = rms_inverse(squares, width)
        gate_part = jnp.zeros((each * CAP, hidden_size), F32)
        up_part = jnp.zeros((each * CAP, hidden_size), F32)
        for q in range(Q):
            part_q = slice(q * columns, (q + 1) * columns)
            mid = (arrived[q] * inverse * gains[:, part_q]).astype(BF16)
            gate_part += dot(mid, e_gate[part_q, :])
            up_part += dot(mid, e_up[part_q, :])
        hidden = (silu(gate_part) * up_part).astype(BF16)
        for q in range(Q):
            down = dot(hidden, e_down[:, q * columns : (q + 1) * columns])
            for s in range(CAP):
                for t in range(tiles):
                    wide[at(q, s, t), :] = down[
                        s * each : (s + 1) * each, t * LANES : (t + 1) * LANES
                    ]
        back_box[blocks] = (
            wide[base : base + lines, :].astype(BF16).reshape(each * Q, CAP * tiles, LANES)
        )
        with jax.named_scope("back_start"):
            send_part(back_box, got_box, back_send, back_recv, part, -1)
    got_box[tp] = back_box[tp]

    total = residual.astype(F32) + dense_own[tp]
    for u in range(1, Q):
        dense_sums[u - 1].wait_recv()
        total += dense_in[u].astype(F32)
    routed = jnp.zeros((PAD, columns), F32)
    for part in range(PARTS):
        with jax.named_scope("back_wait"):
            whole_part(back_box, got_box, back_send, back_recv, part).wait_recv()
        base = part * lines
        blocks = pl.ds(part * each * Q, each * Q)
        wide_got[base : base + lines, :] = got_box[blocks].reshape(lines, LANES).astype(F32)
        results = jnp.concatenate(
            [wide_got[pl.ds(base + t, rows, stride=tiles), :] for t in range(tiles)], axis=1
        ).astype(BF16)
        some_slots = slice(part * rows, (part + 1) * rows)
        routed += dot(high[:, some_slots], results) + dot(low[:, some_slots], results)
    final[tp] = (total + routed[:count, :]).astype(BF16)
    with jax.named_scope("gather"):
        last = [to_peer(3, u, final.at[tp], final.at[tp]) for u in range(1, Q)]
        for copy in last:
            copy.start()
        for copy in last:
            copy.wait_recv()
    for q in range(Q):
        new_tokens[:, q * columns : (q + 1) * columns] = final[q]
    for copy in sums + spread + dense_sums + last:
        copy.wait_send()
    for part in range(PARTS):
        whole_part(out_box, in_box, go_send, go_recv, part).wait_send()
        whole_part(back_box, got_box, back_send, back_recv, part).wait_send()
    for back in backs:
        back.wait()


def hand_on_kernel(tokens_h, state, new_tokens, new_state, rows, held, sem_in, sem_out):
    chunk = state.shape[0] // (sem_in.shape[0] - 1)
    pairs = [(tokens_h, rows, new_tokens)] + [
        (state.at[pl.ds(c, chunk)], held.at[pl.ds(c, chunk)], new_state.at[pl.ds(c, chunk)])
        for c in range(0, state.shape[0], chunk)
    ]
    ins = fetch([(src, mid) for src, mid, _ in pairs], sem_in)
    outs = []
    for i, (_, mid, dst) in enumerate(pairs):
        ins[i].wait()
        outs.append(pltpu.make_async_copy(mid, dst, sem_out.at[i]))
        outs[-1].start()
    for copy in outs:
        copy.wait()


def shards(
    tokens, delta_state, first_gain, query_weight, key_weight, value_weight, outgate_weight,
    beta_weight, decay_weight, decay_rate, decay_bias, head_gain, out_weight, second_gain,
    blend_weight, dense_gate_weight, dense_up_weight, dense_down_weight,
    expert_gate, expert_up, expert_down, route_ids, route_weights,
):
    count, width = tokens.shape
    heads, size = delta_state.shape[1], delta_state.shape[2]
    groups = lax.axis_size("ep")
    columns = width // Q
    hidden = dense_gate_weight.shape[1]
    expert_hidden = expert_gate.shape[2]
    anywhere = pl.BlockSpec(memory_space=pl.ANY)
    near = pl.BlockSpec(memory_space=VMEM)
    wire = VMEM((Q, count, columns), BF16)
    lines = groups * Q * CAP * columns // LANES
    box = VMEM((groups * Q, CAP * columns // LANES, LANES), BF16)
    wide = VMEM((lines, LANES), F32)
    new_tokens, new_state = pl.pallas_call(
        layer_kernel,
        out_shape=(
            jax.ShapeDtypeStruct((count, width), BF16),
            jax.ShapeDtypeStruct(delta_state.shape, F32),
        ),
        in_specs=[anywhere] * 23,
        out_specs=(near, anywhere),
        scratch_shapes=[
            VMEM((count, width), BF16),
            VMEM((width // 128, 128), BF16),
            VMEM((8, width), BF16),
            VMEM((8, width), BF16),
            VMEM((1, 8), F32),
            VMEM((1, 8), F32),
            VMEM((1, size), BF16),
            VMEM((width // 128, 128), BF16),
            VMEM((width // 128, 128), BF16),
            VMEM(route_ids.shape[::-1], jnp.int32),
            VMEM(route_ids.shape[::-1], F32),
            VMEM((4, width, heads * size), BF16),
            VMEM((heads * size, width), BF16),
            VMEM(delta_state.shape, F32),
            VMEM((count, heads * size), F32),
            VMEM((width, hidden), BF16),
            VMEM((width, hidden), BF16),
            VMEM((hidden, width), BF16),
            VMEM((width, expert_hidden), BF16),
            VMEM((width, expert_hidden), BF16),
            VMEM((expert_hidden, width), BF16),
            wire, wire, wire, wire, wire, wire,
            VMEM((PAD, columns), BF16),
            VMEM((count, width), BF16),
            box, box, wide, wide, wide, box, box,
            VMEM((Q, count, columns), F32),
            pltpu.SemaphoreType.DMA((11,)),
            pltpu.SemaphoreType.DMA((5,)),
            pltpu.SemaphoreType.DMA((6,)),
            pltpu.SemaphoreType.DMA((6,)),
            pltpu.SemaphoreType.DMA((6,)),
            pltpu.SemaphoreType.DMA((4, Q)),
            pltpu.SemaphoreType.DMA((4, Q)),
            pltpu.SemaphoreType.DMA((PARTS,)),
            pltpu.SemaphoreType.DMA((PARTS,)),
            pltpu.SemaphoreType.DMA((PARTS,)),
            pltpu.SemaphoreType.DMA((PARTS,)),
        ],
        compiler_params=pltpu.CompilerParams(
            collective_id=0, has_side_effects=True, vmem_limit_bytes=67043328
        ),
        name="layer",
    )(
        tokens, first_gain.reshape(-1, 128), beta_weight.T, decay_weight.T, decay_rate[None],
        decay_bias[None], head_gain[None], second_gain.reshape(-1, 128), blend_weight.reshape(-1, 128),
        route_ids.T, route_weights.T,
        query_weight, key_weight, value_weight, outgate_weight, out_weight, delta_state,
        dense_gate_weight, dense_up_weight, dense_down_weight,
        expert_gate, expert_up, expert_down,
    )
    return pl.pallas_call(
        hand_on_kernel,
        out_shape=(
            jax.ShapeDtypeStruct((count, width), BF16),
            jax.ShapeDtypeStruct(delta_state.shape, F32),
        ),
        in_specs=[anywhere] * 2,
        out_specs=(anywhere, anywhere),
        scratch_shapes=[
            VMEM((count, width), BF16),
            VMEM(delta_state.shape, F32),
            pltpu.SemaphoreType.DMA((7,)),
            pltpu.SemaphoreType.DMA((7,)),
        ],
        compiler_params=pltpu.CompilerParams(vmem_limit_bytes=67043328),
        name="hand_on",
    )(new_tokens, new_state)


def solution(mesh):
    placed = (
        P("ep", None),
        P("ep", "tp", None, None),
        P(),
        P(None, "tp"),
        P(None, "tp"),
        P(None, "tp"),
        P(None, "tp"),
        P(),
        P(),
        P(),
        P(),
        P(),
        P("tp", None),
        P(),
        P(),
        P(None, "tp"),
        P(None, "tp"),
        P("tp", None),
        P(("ep", "tp"), None, None),
        P(("ep", "tp"), None, None),
        P(("ep", "tp"), None, None),
        P("ep", None),
        P("ep", None),
    )
    return jax.shard_map(
        shards,
        mesh=mesh,
        in_specs=placed,
        out_specs=(P("ep", None), P("ep", "tp", None, None)),
        check_vma=False,
    )
```

time: 60.4 us -> 53.9 us (0.89)
  local copies, waits for them, and re-layouts: 5.45 us -> 0 us
  Pallas kernels: 54.1 us -> 53.1 us
    unnamed x2 -> x0, local copies, waits for them, and re-layouts: 5.45 us -> none
    pallas_call x1, Pallas kernels: 54.1 us -> 50.3 us  [shards(): pl.pallas_call(layer_kernel, out_shape=(jax.ShapeDtypeStruct((count, widt...]
    pallas_call x0 -> x1, Pallas kernels: none -> 2.88 us  [shards(): pl.pallas_call(hand_on_kernel, out_shape=(jax.ShapeDtypeStruct((count, wi...]
where the time goes in v4:
time: 53.9 us; the launch traced here: 53.8 us
  Pallas kernels  53.1 us (99%)
  between operations  0.65 us (1%)
    pallas_call x1, Pallas kernels, shards(): pl.pallas_call(layer_kernel, out_shape=(jax.ShapeDtypeStruct((count, widt...  50.3 us
    pallas_call x1, Pallas kernels, shards(): pl.pallas_call(hand_on_kernel, out_shape=(jax.ShapeDtypeStruct((count, wi...  2.88 us

profile of v4, /device:TPU:1, one launch (start us, length us, event | category | flops | bytes accessed | tf_op | source)
XLA Modules:
  0.0 53.8 jit_solution(4515754200104915036)
XLA Ops:
  0.6 50.3 %layer.1 = (bf16[24,2048]{1,0:T(8,128)(2,1)}, f32[24,2,128,128]{3,2,1,0:T(8,128)}) custom-call(bf16[24,2048]{1,0:T(8,128)(2,1)} %tokens_h.1, bf16[16,128]{1,0:T(8,128)(2,1)} %bitcast.12, bf16[8,2048]{1,0:T(8,128)(2,1)} %bitcast.10, bf16[8,2048]{1,0:T(8,128)(2,1)} %bitcast.11, f32[1,8]{1,0:T(1,128)} %bitcast.17, f32[1,8]{1,0:T(1,128)} %bitcast.18, ...), custom_call_target="tpu_custom_call" | custom-call | tf_op jit(solution)/shard_map/layer/pallas_call | solution.py:478
  50.9 2.9 %hand_on.1 = (bf16[24,2048]{1,0:T(8,128)(2,1)}, f32[24,2,128,128]{3,2,1,0:T(8,128)}) custom-call(bf16[24,2048]{1,0:T(8,128)(2,1)} %get-tuple-element.4.tokens_h, f32[24,2,128,128]{3,2,1,0:T(8,128)} %get-tuple-element.5.state), custom_call_target="tpu_custom_call" | custom-call | tf_op jit(solution)/shard_map/hand_on/pallas_call | solution.py:537

commit v5 on v4

--- a/solution.py
+++ b/solution.py
@@ -16,7 +16,13 @@
 LANES = 128
 PAD = 32
 CAP = 2
-PARTS = 4
+PLANE = 8
+STEPS = (0, 1, 7, 2, 6, 3, 5, 4)
+NEAR = 3
+FAR = len(STEPS) - NEAR
+PARTS = ((0, 3), (3, 5), (5, 8))
+PART_OF = [n for n, (lo, hi) in enumerate(PARTS) for _ in range(lo, hi)]
+FFN_ORDER = (1, 2, 0)
 
 
 def silu(x):
@@ -139,8 +145,9 @@
     weights, out_weights, held, read,
     w_gate, w_up, w_down, e_gate, e_up, e_down,
     mixed, mixed_in, pieces_mid, dense_part, dense_in, final,
+    meta, far_meta, far_rows, far_part, far_in,
     rows_mid, full_mid, out_box, in_box, wide_out, wide, wide_got, back_box, got_box, dense_own,
-    small_sem, in_sem, state_sem, back_sem, w_sem, near_send, near_recv, go_send, go_recv, back_send, back_recv,
+    small_sem, in_sem, state_sem, back_sem, w_sem, near_send, near_recv, far_send, far_recv, go_send, go_recv, back_send, back_recv,
 ):
     groups = lax.axis_size("ep")
     ep, tp = lax.axis_index("ep"), lax.axis_index("tp")
@@ -148,7 +155,8 @@
     columns = width // Q
     tiles = columns // LANES
     hidden_size = w_gate.shape[1]
-    each = groups // PARTS
+    plane, spot = ep // PLANE, lax.rem(ep, PLANE)
+    planes = groups // PLANE
 
     small = fetch(
         (
@@ -170,16 +178,6 @@
     mix_loads = fetch(
         [(w, weights.at[i]) for i, w in enumerate((key_w, value_w, query_w, gate_w))], in_sem
     )
-    pieces = fetch(
-        [
-            (state.at[pl.ds(c, chunk)], held.at[pl.ds(c, chunk)])
-            for c in range(0, count, chunk)
-        ],
-        state_sem,
-    )
-    out_load = pltpu.make_async_copy(out_w, out_weights, in_sem.at[4])
-    out_load.start()
-
     barrier = pltpu.get_barrier_semaphore()
 
     def greet(i, carry):
@@ -201,7 +199,33 @@
             device_id=(ep, lax.rem(tp + u, Q)), device_id_type=MESH,
         )
 
-    slots = groups * Q * CAP
+    def to_far(n, f, sign, source, target):
+        there = lax.rem(plane + planes + sign * STEPS[NEAR + f], planes)
+        return pltpu.make_async_remote_copy(
+            src_ref=source, dst_ref=target,
+            send_sem=far_send.at[n, f], recv_sem=far_recv.at[n, f],
+            device_id=(there * PLANE + spot, tp), device_id_type=MESH,
+        )
+
+    def routes(named, weight, row):
+        a = lax.broadcasted_iota(jnp.int32, (LANES, LANES), 0)
+        b = lax.broadcasted_iota(jnp.int32, (LANES, LANES), 1)
+        rank = dot(named.astype(BF16), (a < b).astype(F32).astype(BF16))
+        taken = (named > 0.5) & (rank == lax.rem(row, CAP).astype(F32))
+        pick = jnp.where(taken, 1.0, 0.0).astype(BF16)[:, :PAD]
+        weight = jnp.transpose(jnp.where(taken, weight, 0.0))[:PAD, :]
+        high = weight.astype(BF16)
+        return pick, high, (weight - high.astype(F32)).astype(BF16)
+
+    def named_by(ids_f, scale_f, expert):
+        named = jnp.zeros((expert.shape[0], LANES), F32)
+        weight = jnp.zeros((expert.shape[0], LANES), F32)
+        for k in range(ids.shape[0]):
+            hit = ids_f[k : k + 1, :] == expert
+            named = jnp.where(hit, 1.0, named)
+            weight = jnp.where(hit, scale_f[k : k + 1, :], weight)
+        return named, weight
+
     loads = []
 
     def fetch_rest():
@@ -233,28 +257,32 @@
             ],
             axis=1,
         )
-        row = lax.broadcasted_iota(jnp.int32, (slots, 1), 0)
-        block = row // (Q * CAP)
-        offset = lax.rem(block, each) * PARTS + block // each
-        expert = lax.rem(ep + offset, groups) * Q + lax.rem(row // CAP, Q)
-        named = jnp.zeros((slots, LANES), F32)
-        weight = jnp.zeros((slots, LANES), F32)
-        for k in range(k_count):
-            hit = ids_c[k : k + 1, :] == expert
-            named = jnp.where(hit, 1.0, named)
-            weight = jnp.where(hit, scale_c[k : k + 1, :], weight)
-        a = lax.broadcasted_iota(jnp.int32, (LANES, LANES), 0)
-        b = lax.broadcasted_iota(jnp.int32, (LANES, LANES), 1)
-        rank = dot(named.astype(BF16), (a < b).astype(F32).astype(BF16))
-        taken = (named > 0.5) & (rank == lax.rem(row, CAP).astype(F32))
-        pick = jnp.where(taken, 1.0, 0.0).astype(BF16)[:, :PAD]
-        weight = jnp.transpose(jnp.where(taken, weight, 0.0))[:PAD, :]
-        high = weight.astype(BF16)
-        low = (weight - high.astype(F32)).astype(BF16)
+        ids_f = ids_c.astype(F32)
+        meta[...] = jnp.full(meta.shape, -1.0, F32)
+        meta[:k_count, :] = ids_f
+        meta[8 : 8 + k_count, :] = scale_c
+        row = lax.broadcasted_iota(jnp.int32, (NEAR * PLANE * Q * CAP, 1), 0)
+        at_step = row // (PLANE * Q * CAP)
+        up = jnp.zeros_like(row)
+        for k in range(NEAR):
+            up = jnp.where(at_step == k, STEPS[k], up)
+        there = lax.rem(spot + lax.rem(row // (Q * CAP), PLANE), PLANE)
+        lane = lax.rem(row // CAP, Q)
+        expert = ((lax.rem(plane + up, planes) * PLANE + there) * Q + lane).astype(F32)
+        pick, high, low = routes(*named_by(ids_f, scale_c, expert), row)
         rows_mid[...] = jnp.zeros_like(rows_mid)
     with jax.named_scope("small"):
         for copy in small[2:]:
             copy.wait()
+        pieces = fetch(
+            [
+                (state.at[pl.ds(c, chunk)], held.at[pl.ds(c, chunk)])
+                for c in range(0, count, chunk)
+            ],
+            state_sem,
+        )
+        out_load = pltpu.make_async_copy(out_w, out_weights, in_sem.at[4])
+        out_load.start()
     with jax.named_scope("mixer"):
         backs = mixer(
             tokens, first_gain, beta_t, decay_t, rate, bias, head_gain,
@@ -263,6 +291,9 @@
         )
     with jax.named_scope("barrier"):
         pl.semaphore_wait(barrier, groups - 1 + Q - 1)
+        metas = [to_far(0, f, 1, meta, far_meta.at[f]) for f in range(FAR)]
+        for copy in metas:
+            copy.start()
 
     with jax.named_scope("mix_sum"):
         sums = [to_peer(0, u, mixed.at[lax.rem(tp + u, Q)], mixed_in.at[u]) for u in range(1, Q)]
@@ -277,55 +308,88 @@
         rows_mid[:count, :] = residual
         pieces_mid[tp] = residual
 
-    def send_part(source, target, send_sem, recv_sem, part, sign):
+    def send_step(source, target, send_sem, recv_sem, k, sign):
+        inside = k == 0 or k >= NEAR
+        there = plane if inside else lax.rem(plane + planes + sign * STEPS[k], planes)
+
         def one(place, group, lane):
             pltpu.make_async_remote_copy(
                 src_ref=source.at[place * Q + lane], dst_ref=target.at[place * Q + tp],
-                send_sem=send_sem.at[part], recv_sem=recv_sem.at[part],
+                send_sem=send_sem.at[PART_OF[k]], recv_sem=recv_sem.at[PART_OF[k]],
                 device_id=(group, lane), device_id_type=MESH,
             ).start()
 
         def some(j, carry):
-            group = lax.rem(ep + groups + sign * (j * PARTS + part), groups)
+            group = there * PLANE + lax.rem(spot + PLANE + sign * j, PLANE)
             for lane in range(Q):
-                one(part * each + j, group, lane)
+                one(k * PLANE + j, group, lane)
             return carry
 
-        if part == 0:
+        if inside:
             for u in range(1, Q):
-                one(0, ep, lax.rem(tp + u, Q))
-        lax.fori_loop(1 if part == 0 else 0, each, some, 0)
+                one(k * PLANE, ep, lax.rem(tp + u, Q))
+        lax.fori_loop(1 if inside else 0, PLANE, some, 0)
+
+    def keep(source, target, k):
+        if k == 0 or k >= NEAR:
+            target[k * PLANE * Q + tp] = source[k * PLANE * Q + tp]
 
     def whole_part(source, target, send_sem, recv_sem, part):
-        first = 1 if part == 0 else 0
-        blocks = pl.ds(part * each * Q + first, each * Q - first)
+        lo, hi = PARTS[part]
+        first = sum(k == 0 or k >= NEAR for k in range(lo, hi))
+        blocks = pl.ds(lo * PLANE * Q + first, (hi - lo) * PLANE * Q - first)
         return pltpu.make_async_remote_copy(
             src_ref=source.at[blocks], dst_ref=target.at[blocks],
             send_sem=send_sem.at[part], recv_sem=recv_sem.at[part],
             device_id=(ep, lax.rem(tp + 1, Q)), device_id_type=MESH,
         )
 
-    rows = each * Q * CAP
-    lines = rows * tiles
+    def pack(table, values, k, steps):
+        n = steps * PLANE * Q
+        base = k * PLANE * Q * CAP * tiles
+        outgoing = dot(table, values)
+        for t in range(tiles):
+            wide_out[pl.ds(base + t, n * CAP, stride=tiles), :] = outgoing[
+                :, t * LANES : (t + 1) * LANES
+            ]
+        out_box[pl.ds(k * PLANE * Q, n)] = (
+            wide_out[base : base + n * CAP * tiles, :].astype(BF16).reshape(n, CAP * tiles, LANES)
+        )
+
+    def unpack(k, steps):
+        n = steps * PLANE * Q
+        base = k * PLANE * Q * CAP * tiles
+        wide_got[base : base + n * CAP * tiles, :] = (
+            got_box[pl.ds(k * PLANE * Q, n)].reshape(n * CAP * tiles, LANES).astype(F32)
+        )
+        return jnp.concatenate(
+            [wide_got[pl.ds(base + t, n * CAP, stride=tiles), :] for t in range(tiles)], axis=1
+        ).astype(BF16)
+
+    step_slots = PLANE * Q * CAP
     x = rows_mid[...]
     with jax.named_scope("go_start"):
-        for part in range(PARTS):
-            base = part * lines
-            outgoing = dot(pick[part * rows : (part + 1) * rows, :], x)
-            for t in range(tiles):
-                wide_out[pl.ds(base + t, rows, stride=tiles), :] = outgoing[
-                    :, t * LANES : (t + 1) * LANES
-                ]
-            blocks = pl.ds(part * each * Q, each * Q)
-            out_box[blocks] = (
-                wide_out[base : base + lines, :].astype(BF16).reshape(each * Q, CAP * tiles, LANES)
-            )
-            send_part(out_box, in_box, go_send, go_recv, part, 1)
-            if part == 0:
-                spread = [to_peer(1, u, pieces_mid.at[tp], pieces_mid.at[tp]) for u in range(1, Q)]
-                for copy in spread:
-                    copy.start()
-    in_box[tp] = out_box[tp]
+        spread = [to_peer(1, u, pieces_mid.at[tp], pieces_mid.at[tp]) for u in range(1, Q)]
+        fars = [to_far(1, f, 1, pieces_mid.at[tp], far_rows.at[f]) for f in range(FAR)]
+        for copy in spread + fars:
+            copy.start()
+        for k in range(NEAR):
+            pack(pick[k * step_slots : (k + 1) * step_slots, :], x, k, 1)
+            send_step(out_box, in_box, go_send, go_recv, k, 1)
+        keep(out_box, in_box, 0)
+    with jax.named_scope("far_tables"):
+        row = lax.broadcasted_iota(jnp.int32, (PLANE * Q * CAP, 1), 0)
+        there = lax.rem(spot + row // (Q * CAP), PLANE)
+        expert = ((plane * PLANE + there) * Q + lax.rem(row // CAP, Q)).astype(F32)
+        found = []
+        for f in range(FAR):
+            metas[f].wait_recv()
+            found.append(named_by(far_meta[f, 0:8, :], far_meta[f, 8:16, :], expert))
+        far_pick, far_high, far_low = routes(
+            jnp.concatenate([n for n, _ in found], axis=0),
+            jnp.concatenate([w for _, w in found], axis=0),
+            lax.broadcasted_iota(jnp.int32, (FAR * PLANE * Q * CAP, 1), 0),
+        )
 
     gains = row_of(gain[...].astype(F32))
     with jax.named_scope("dense"):
@@ -360,12 +424,25 @@
         for n in range(3, 6):
             loads[n].wait()
 
+    with jax.named_scope("relay"):
+        for f in range(FAR):
+            fars[f].wait_recv()
+            values = jnp.concatenate(
+                [far_rows[f], jnp.zeros((PAD - count, columns), BF16)], axis=0
+            )
+            pack(far_pick[f * step_slots : (f + 1) * step_slots, :], values, NEAR + f, 1)
+            send_step(out_box, in_box, go_send, go_recv, NEAR + f, 1)
+            keep(out_box, in_box, NEAR + f)
+
     apart = Q * CAP * tiles
-    for part in range(PARTS):
+    for part in FFN_ORDER:
         with jax.named_scope("go_wait"):
             whole_part(out_box, in_box, go_send, go_recv, part).wait_recv()
-        blocks = pl.ds(part * each * Q, each * Q)
-        base = part * lines
+        lo, hi = PARTS[part]
+        each = (hi - lo) * PLANE
+        lines = each * apart
+        blocks = pl.ds(lo * PLANE * Q, each * Q)
+        base = lo * PLANE * apart
         wide[base : base + lines, :] = in_box[blocks].reshape(lines, LANES).astype(F32)
 
         def at(q, s, t):
@@ -404,25 +481,38 @@
             wide[base : base + lines, :].astype(BF16).reshape(each * Q, CAP * tiles, LANES)
         )
         with jax.named_scope("back_start"):
-            send_part(back_box, got_box, back_send, back_recv, part, -1)
-    got_box[tp] = back_box[tp]
+            for k in range(lo, hi):
+                send_step(back_box, got_box, back_send, back_recv, k, -1)
+                keep(back_box, got_box, k)
 
     total = residual.astype(F32) + dense_own[tp]
     for u in range(1, Q):
         dense_sums[u - 1].wait_recv()
         total += dense_in[u].astype(F32)
+    homes = [to_far(2, f, -1, far_part.at[f], far_in.at[f]) for f in range(FAR)]
     routed = jnp.zeros((PAD, columns), F32)
-    for part in range(PARTS):
+
+    def wait_back(part):
         with jax.named_scope("back_wait"):
             whole_part(back_box, got_box, back_send, back_recv, part).wait_recv()
-        base = part * lines
-        blocks = pl.ds(part * each * Q, each * Q)
-        wide_got[base : base + lines, :] = got_box[blocks].reshape(lines, LANES).astype(F32)
-        results = jnp.concatenate(
-            [wide_got[pl.ds(base + t, rows, stride=tiles), :] for t in range(tiles)], axis=1
-        ).astype(BF16)
-        some_slots = slice(part * rows, (part + 1) * rows)
-        routed += dot(high[:, some_slots], results) + dot(low[:, some_slots], results)
+
+    for part in FFN_ORDER:
+        wait_back(part)
+        for k in range(*PARTS[part]):
+            results = unpack(k, 1)
+            if k < NEAR:
+                some_slots = slice(k * step_slots, (k + 1) * step_slots)
+                routed += dot(high[:, some_slots], results) + dot(low[:, some_slots], results)
+                continue
+            f = k - NEAR
+            some_slots = slice(f * step_slots, (f + 1) * step_slots)
+            far = dot(far_high[:, some_slots], results) + dot(far_low[:, some_slots], results)
+            far_part[f] = far[:count, :].astype(BF16)
+            homes[f].start()
+    with jax.named_scope("far_wait"):
+        for f in range(FAR):
+            homes[f].wait_recv()
+            total += far_in[f].astype(F32)
     final[tp] = (total + routed[:count, :]).astype(BF16)
     with jax.named_scope("gather"):
         last = [to_peer(3, u, final.at[tp], final.at[tp]) for u in range(1, Q)]
@@ -432,9 +522,9 @@
             copy.wait_recv()
     for q in range(Q):
         new_tokens[:, q * columns : (q + 1) * columns] = final[q]
-    for copy in sums + spread + dense_sums + last:
+    for copy in sums + spread + dense_sums + last + metas + fars + homes:
         copy.wait_send()
-    for part in range(PARTS):
+    for part in range(len(PARTS)):
         whole_part(out_box, in_box, go_send, go_recv, part).wait_send()
         whole_part(back_box, got_box, back_send, back_recv, part).wait_send()
     for back in backs:
@@ -506,6 +596,11 @@
             VMEM((width, expert_hidden), BF16),
             VMEM((expert_hidden, width), BF16),
             wire, wire, wire, wire, wire, wire,
+            VMEM((16, LANES), F32),
+            VMEM((FAR, 16, LANES), F32),
+            VMEM((FAR, count, columns), BF16),
+            VMEM((FAR, count, columns), BF16),
+            VMEM((FAR, count, columns), BF16),
             VMEM((PAD, columns), BF16),
             VMEM((count, width), BF16),
             box, box, wide, wide, wide, box, box,
@@ -517,10 +612,12 @@
             pltpu.SemaphoreType.DMA((6,)),
             pltpu.SemaphoreType.DMA((4, Q)),
             pltpu.SemaphoreType.DMA((4, Q)),
-            pltpu.SemaphoreType.DMA((PARTS,)),
-            pltpu.SemaphoreType.DMA((PARTS,)),
-            pltpu.SemaphoreType.DMA((PARTS,)),
-            pltpu.SemaphoreType.DMA((PARTS,)),
+            pltpu.SemaphoreType.DMA((3, FAR)),
+            pltpu.SemaphoreType.DMA((3, FAR)),
+            pltpu.SemaphoreType.DMA((len(PARTS),)),
+            pltpu.SemaphoreType.DMA((len(PARTS),)),
+            pltpu.SemaphoreType.DMA((len(PARTS),)),
+            pltpu.SemaphoreType.DMA((len(PARTS),)),
         ],
         compiler_params=pltpu.CompilerParams(
             collective_id=0, has_side_effects=True, vmem_limit_bytes=67043328

time: 53.9 us -> 51.8 us (0.961)
  Pallas kernels: 53.1 us -> 51 us
    pallas_call x1, Pallas kernels: 50.3 us -> 48.2 us  [shards(): pl.pallas_call(layer_kernel, out_shape=(jax.ShapeDtypeStruct((count, widt...]
where the time goes in v5:
time: 51.8 us; the launch traced here: 51.7 us
  Pallas kernels  51 us (98%)
  between operations  0.65 us (1%)
    pallas_call x1, Pallas kernels, shards(): pl.pallas_call(layer_kernel, out_shape=(jax.ShapeDtypeStruct((count, widt...  48.2 us
    pallas_call x1, Pallas kernels, shards(): pl.pallas_call(hand_on_kernel, out_shape=(jax.ShapeDtypeStruct((count, wi...  2.88 us

profile of v5, /device:TPU:1, one launch (start us, length us, event | category | flops | bytes accessed | tf_op | source)
XLA Modules:
  0.0 51.7 jit_solution(7761110029298926061)
XLA Ops:
  0.6 48.2 %layer.1 = (bf16[24,2048]{1,0:T(8,128)(2,1)}, f32[24,2,128,128]{3,2,1,0:T(8,128)}) custom-call(bf16[24,2048]{1,0:T(8,128)(2,1)} %tokens_h.1, bf16[16,128]{1,0:T(8,128)(2,1)} %bitcast.12, bf16[8,2048]{1,0:T(8,128)(2,1)} %bitcast.10, bf16[8,2048]{1,0:T(8,128)(2,1)} %bitcast.11, f32[1,8]{1,0:T(1,128)} %bitcast.17, f32[1,8]{1,0:T(1,128)} %bitcast.18, ...), custom_call_target="tpu_custom_call" | custom-call | tf_op jit(solution)/shard_map/layer/pallas_call | solution.py:568
  48.8 2.9 %hand_on.1 = (bf16[24,2048]{1,0:T(8,128)(2,1)}, f32[24,2,128,128]{3,2,1,0:T(8,128)}) custom-call(bf16[24,2048]{1,0:T(8,128)(2,1)} %get-tuple-element.4.tokens_h, f32[24,2,128,128]{3,2,1,0:T(8,128)} %get-tuple-element.5.state), custom_call_target="tpu_custom_call" | custom-call | tf_op jit(solution)/shard_map/hand_on/pallas_call | solution.py:634

commit v6 on v5

--- a/solution.py
+++ b/solution.py
@@ -18,11 +18,11 @@
 CAP = 2
 PLANE = 8
 STEPS = (0, 1, 7, 2, 6, 3, 5, 4)
-NEAR = 3
+NEAR = 5
 FAR = len(STEPS) - NEAR
 PARTS = ((0, 3), (3, 5), (5, 8))
 PART_OF = [n for n, (lo, hi) in enumerate(PARTS) for _ in range(lo, hi)]
-FFN_ORDER = (1, 2, 0)
+FFN_ORDER = (0, 2, 1)
 
 
 def silu(x):
@@ -496,7 +496,7 @@
         with jax.named_scope("back_wait"):
             whole_part(back_box, got_box, back_send, back_recv, part).wait_recv()
 
-    for part in FFN_ORDER:
+    for part in sorted(FFN_ORDER, key=lambda part: PARTS[part][0] < NEAR):
         wait_back(part)
         for k in range(*PARTS[part]):
             results = unpack(k, 1)
@@ -642,8 +642,8 @@
         scratch_shapes=[
             VMEM((count, width), BF16),
             VMEM(delta_state.shape, F32),
-            pltpu.SemaphoreType.DMA((7,)),
-            pltpu.SemaphoreType.DMA((7,)),
+            pltpu.SemaphoreType.DMA((13,)),
+            pltpu.SemaphoreType.DMA((13,)),
         ],
         compiler_params=pltpu.CompilerParams(vmem_limit_bytes=67043328),
         name="hand_on",

time: 51.8 us -> 51.1 us (0.986)
  Pallas kernels: 51 us -> 50.4 us
    pallas_call x1, Pallas kernels: 48.2 us -> 47.5 us  [shards(): pl.pallas_call(layer_kernel, out_shape=(jax.ShapeDtypeStruct((count, widt...]
where the time goes in v6:
time: 51.1 us; the launch traced here: 51 us
  Pallas kernels  50.4 us (99%)
  between operations  0.65 us (1%)
    pallas_call x1, Pallas kernels, shards(): pl.pallas_call(layer_kernel, out_shape=(jax.ShapeDtypeStruct((count, widt...  47.5 us
    pallas_call x1, Pallas kernels, shards(): pl.pallas_call(hand_on_kernel, out_shape=(jax.ShapeDtypeStruct((count, wi...  2.88 us

profile of v6, /device:TPU:1, one launch (start us, length us, event | category | flops | bytes accessed | tf_op | source)
XLA Modules:
  0.0 51.0 jit_solution(11398797404679682684)
XLA Ops:
  0.6 47.5 %layer.1 = (bf16[24,2048]{1,0:T(8,128)(2,1)}, f32[24,2,128,128]{3,2,1,0:T(8,128)}) custom-call(bf16[24,2048]{1,0:T(8,128)(2,1)} %tokens_h.1, bf16[16,128]{1,0:T(8,128)(2,1)} %bitcast.12, bf16[8,2048]{1,0:T(8,128)(2,1)} %bitcast.10, bf16[8,2048]{1,0:T(8,128)(2,1)} %bitcast.11, f32[1,8]{1,0:T(1,128)} %bitcast.17, f32[1,8]{1,0:T(1,128)} %bitcast.18, ...), custom_call_target="tpu_custom_call" | custom-call | tf_op jit(solution)/shard_map/layer/pallas_call | solution.py:568
  48.1 2.9 %hand_on.1 = (bf16[24,2048]{1,0:T(8,128)(2,1)}, f32[24,2,128,128]{3,2,1,0:T(8,128)}) custom-call(bf16[24,2048]{1,0:T(8,128)(2,1)} %get-tuple-element.4.tokens_h, f32[24,2,128,128]{3,2,1,0:T(8,128)} %get-tuple-element.5.state), custom_call_target="tpu_custom_call" | custom-call | tf_op jit(solution)/shard_map/hand_on/pallas_call | solution.py:634
